TPU v7x, 256 devices: a whole 4x4x8 slice. The times are simulated.
256 devices in a mesh: sp: 64 (over z, x, core), tp: 4 (over y).
Axes of the slice: x: 4, y: 4, z: 8, core: 2. Of those that a mesh axis runs over, the one named last changes fastest.
Arguments:
- queries: bfloat16 [8192, 1024], P('sp', 'tp'), may hold values from -160 to 160
- keys: bfloat16 [8192, 256], P('sp', 'tp'), may hold values from -5 to 5
- values: bfloat16 [8192, 256], P('sp', 'tp'), may hold values from -6 to 6
- cum_gate: float32 [8192, 16], P('sp', 'tp'), as said below
- doc_ids: int32 [8192], P('sp'), may hold values from 0 to 7, never falling along the last dimension, each value on 1 to 4224 neighbouring positions
- residual: bfloat16 [8192, 2048], P(('sp', 'tp')), may hold values from -6 to 6
- out_proj: bfloat16 [1024, 2048], replicated, may hold values from -0.1875 to 0.1875
- norm_gain: float32 [2048], replicated, may hold values from 0.1 to 1.9
- route_ids: int32 [8192, 2], P(('sp', 'tp')), may hold values from 0 to 63, all different within a row; in each aligned block of 32 rows (0 to 31, 32 to 63, ...) at most 2 rows name the same one
- route_weights: float32 [8192, 2], P(('sp', 'tp')), may hold values from 0.2 to 1
- expert_gate: bfloat16 [64, 2048, 1024], P('sp', None, 'tp'), may hold values from -0.125 to 0.125
- expert_up: bfloat16 [64, 2048, 1024], P('sp', None, 'tp'), may hold values from -0.125 to 0.125
- expert_down: bfloat16 [64, 1024, 2048], P('sp', 'tp'), may hold values from -0.1875 to 0.1875
Outputs:
- mixed: bfloat16 [8192, 2048], P(('sp', 'tp'))
Inputs may be any that keep to these rules, and one draw needn't show every extreme that they name: `route_ids`: within each aligned block of 32 rows no expert is named by more than 2 rows, and in every draw some block has an expert named by exactly 2 rows; the 2 experts of a row differ. `doc_ids`: never falling along positions; a document spans at most 4224 positions, and one spans exactly that many. `cum_gate`: never rising along positions.
All inputs are finite; a program needn't handle non-finite values.
Results may differ from a plain program's by a relative error of at most 0.014.
Values may be sent and summed in bfloat16 or wider, within the bound.
A program may use at most 128 MiB of HBM per device.

v0:
```python
import jax
import jax.numpy as jnp
from jax import lax
from jax.sharding import PartitionSpec as P

D = 2048
HEAD_DIM = 64
TOP = 2


very_low = -1e30
norm_eps = 1e-06


def rows_first(arrays, axis, dims):
    turned = [jnp.moveaxis(a, dim, 0) for a, dim in zip(arrays, dims)]
    both = jnp.concatenate([t.reshape(len(t), -1) for t in turned], axis=1)
    out, at, outs = (lax.all_gather(both, axis, axis=0, tiled=True), 0, [])
    for t, dim in zip(turned, dims):
        section = out[:, at : at + t[0].size].reshape(-1, *t.shape[1:])
        outs.append(jnp.moveaxis(section, 0, dim))
        at += t[0].size
    return tuple(outs)


def in_order(pieces, dim):
    pieces = jnp.moveaxis(pieces, 0, dim)
    dims = pieces.shape
    return pieces.reshape(*dims[:dim], dims[dim] * dims[dim + 1], *dims[dim + 2 :])


def from_everyone(value, axis):
    copies = jnp.broadcast_to(value, (lax.axis_size(axis), *value.shape))
    return lax.all_to_all(copies, axis, split_axis=0, concat_axis=0, tiled=True)


def gather_directly(value, axis, dim):
    return in_order(from_everyone(value, axis), dim)


def in_one_piece(arrays, axis, dim, along):
    widths = [a.shape[along] for a in arrays]
    both = jnp.concatenate(arrays, axis=along)
    out = lax.all_gather(both, axis, axis=dim, tiled=True)
    return tuple(jnp.split(out, [sum(widths[:k]) for k in range(1, len(widths))], axis=along))


def slot_ranks(picked_ids, experts):
    onehot = (picked_ids[..., None] == jnp.arange(experts, dtype=jnp.int32)).astype(jnp.int32)
    earlier = jnp.cumsum(onehot, axis=-2) - onehot
    return jnp.sum(earlier * onehot, axis=-1)


def local(
    queries,
    keys,
    values,
    cum_gate,
    doc_ids,
    residual,
    out_proj,
    norm_gain,
    route_ids,
    route_weights,
    expert_gate,
    expert_up,
    expert_down,
):
    whole_gate, whole_up, whole_down = rows_first(
        (expert_gate, expert_up, expert_down), "tp", (2, 2, 1)
    )
    own_tokens = queries.shape[0]
    head_count = queries.shape[1] // HEAD_DIM
    kv_count = keys.shape[1] // HEAD_DIM
    group_size = head_count // kv_count
    scale = HEAD_DIM ** (-0.5)
    own_start = lax.axis_index("sp") * own_tokens
    query_pos = own_start + jnp.arange(own_tokens, dtype=jnp.int32)
    query_heads = queries.reshape(own_tokens, kv_count, group_size, HEAD_DIM)
    query_gate = cum_gate.reshape(own_tokens, kv_count, group_size)
    gate_all, doc_all = (gather_directly(cum_gate, "sp", 0), gather_directly(doc_ids, "sp", 0))

    def attend(state, key_block, value_block, first, block_len):
        gate_keys = lax.dynamic_slice_in_dim(gate_all, first, block_len, 0)
        doc_keys = lax.dynamic_slice_in_dim(doc_all, first, block_len, 0)
        key_heads = key_block.reshape(block_len, kv_count, HEAD_DIM)
        value_heads = value_block.reshape(block_len, kv_count, HEAD_DIM)
        scores = (
            jnp.einsum("tkgd,skd->tkgs", query_heads, key_heads, preferred_element_type=jnp.float32)
            * scale
        )
        scores = (
            scores
            + query_gate[..., None]
            - gate_keys.T.reshape(kv_count, group_size, block_len)[None]
        )
        key_pos = first + jnp.arange(block_len, dtype=jnp.int32)
        allowed = (key_pos[None, :] <= query_pos[:, None]) & (doc_keys[None, :] == doc_ids[:, None])
        allowed = allowed[:, None, None, :]
        scores = jnp.where(allowed, scores, very_low)
        top_old, total_old, summed_old = state
        top_new = jnp.maximum(top_old, jnp.max(scores, axis=-1))
        weights = jnp.where(allowed, jnp.exp(scores - top_new[..., None]), 0.0)
        fade = jnp.exp(top_old - top_new)
        total_new = total_old * fade + jnp.sum(weights, axis=-1)
        summed_new = summed_old * fade[..., None] + jnp.einsum(
            "tkgs,skd->tkgd",
            weights.astype(jnp.bfloat16),
            value_heads,
            preferred_element_type=jnp.float32,
        )
        return (top_new, total_new, summed_new)

    start_state = (
        jnp.full((own_tokens, kv_count, group_size), very_low, jnp.float32),
        jnp.zeros((own_tokens, kv_count, group_size), jnp.float32),
        jnp.zeros((own_tokens, kv_count, group_size, HEAD_DIM), jnp.float32),
    )
    key_piece, value_piece = in_one_piece((keys, values), "sp", 0, 1)
    piece_len = key_piece.shape[0]
    block_len = min(piece_len, own_tokens)

    def one_block(index, inner):
        offset = index * block_len
        key_block = lax.dynamic_slice_in_dim(key_piece, offset, block_len, 0)
        value_block = lax.dynamic_slice_in_dim(value_piece, offset, block_len, 0)
        last_doc = lax.dynamic_index_in_dim(doc_all, offset + block_len - 1, 0, keepdims=False)
        needed = (offset <= own_start + own_tokens - 1) & (last_doc >= doc_ids[0])
        return lax.cond(
            needed,
            lambda carried: attend(carried, key_block, value_block, offset, block_len),
            lambda carried: carried,
            inner,
        )

    top, total, summed = lax.fori_loop(0, piece_len // block_len, one_block, start_state)
    attended = (
        (summed / total[..., None]).reshape(own_tokens, head_count * HEAD_DIM).astype(jnp.bfloat16)
    )
    tp_count = lax.axis_size("tp")
    sp_count = lax.axis_size("sp")
    rows_dev = residual.shape[0]
    plane_entries = lax.all_to_all(attended, "tp", split_axis=0, concat_axis=1, tiled=True)
    projected = jnp.dot(plane_entries, out_proj, preferred_element_type=jnp.float32)
    stream = (residual.astype(jnp.float32) + projected).astype(jnp.bfloat16)
    stream_f = stream.astype(jnp.float32)
    normed = stream_f * lax.rsqrt(jnp.mean(stream_f * stream_f, axis=1, keepdims=True) + norm_eps)
    normed = (normed * norm_gain[None, :]).astype(jnp.bfloat16)
    exp_dev = expert_gate.shape[0]
    experts = exp_dev * sp_count
    capacity = max(2, 2 * rows_dev * TOP // experts)
    own_flat = route_ids.reshape(-1)
    own_rank = slot_ranks(route_ids.reshape(1, rows_dev * TOP), experts)[0]
    own_dest = own_flat * capacity + own_rank
    row_of = jnp.arange(rows_dev * TOP, dtype=jnp.int32) // TOP
    outgoing = jnp.zeros((experts * capacity, D), jnp.bfloat16).at[own_dest].set(normed[row_of])
    arrived = lax.all_to_all(
        outgoing.reshape(experts, capacity, D), "sp", split_axis=0, concat_axis=1, tiled=True
    )
    gate = jnp.einsum("erd,edf->erf", arrived, whole_gate, preferred_element_type=jnp.float32)
    upper = jnp.einsum("erd,edf->erf", arrived, whole_up, preferred_element_type=jnp.float32)
    hidden = (jax.nn.silu(gate) * upper).astype(jnp.bfloat16)
    group_width = hidden.shape[2] // tp_count
    hidden_groups = hidden.reshape(exp_dev, sp_count * capacity, tp_count, group_width)
    down_groups = whole_down.reshape(exp_dev, tp_count, group_width, D)
    pieces = jnp.einsum(
        "ergf,egfd->egrd", hidden_groups, down_groups, preferred_element_type=jnp.float32
    ).astype(jnp.bfloat16)
    expert_out = jnp.sum(pieces.astype(jnp.float32), axis=1).astype(jnp.bfloat16)
    returned = lax.all_to_all(expert_out, "sp", split_axis=1, concat_axis=0, tiled=True)
    selected = returned.reshape(experts * capacity, D)[own_dest]
    weighted = selected.astype(jnp.float32).reshape(rows_dev, TOP, D) * route_weights[..., None]
    return (stream_f + jnp.sum(weighted, axis=1)).astype(jnp.bfloat16)


def solution(mesh):
    in_specs = (
        P("sp", "tp"),
        P("sp", "tp"),
        P("sp", "tp"),
        P("sp", "tp"),
        P("sp"),
        P(("sp", "tp"), None),
        P(),
        P(),
        P(("sp", "tp"), None),
        P(("sp", "tp"), None),
        P("sp", None, "tp"),
        P("sp", None, "tp"),
        P("sp", "tp", None),
    )
    out_specs = P(("sp", "tp"), None)
    return jax.shard_map(local, mesh=mesh, in_specs=in_specs, out_specs=out_specs, check_vma=False)
```

profile of v0, /device:TPU:1, one launch (start us, length us, event | category | flops | bytes accessed | tf_op | source)
XLA Modules:
  0.0 290.8 jit_solution(12940880266380916190)
XLA Ops:
  6.5 1.4 pad_maximum_fusion.1
  8.0 1.5 copy.48
  9.5 1.5 copy.49
  11.1 1.8 pad_maximum_fusion
  12.9 0.6 broadcast_in_dim.63
  13.5 13.0 %all-to-all-start = ((s32[64,1,128]{2,1,0:T(1,128)}), s32[64,1,128]{2,1,0:T(1,128)S(1)}, u32[]{:S(2)}, u32[]{:S(2)}) async-start(s32[64,1,128]{2,1,0:T(1,128)} %broadcast_in_dim.63), calls=%async_computation | async-start | bytes 65536 | tf_op jit(solution)/shard_map/all_to_all | solution.py:34
  27.4 8.5 %all-to-all-done = s32[64,1,128]{2,1,0:T(1,128)S(1)} async-done(((s32[64,1,128]{2,1,0:T(1,128)}), s32[64,1,128]{2,1,0:T(1,128)S(1)}, u32[]{:S(2)}, u32[]{:S(2)}) %all-to-all-start) | async-done | bytes 32800 | tf_op jit(solution)/shard_map/all_to_all | solution.py:34
  35.9 0.7 broadcast_in_dim.64
  36.6 4.7 %all-to-all-start.1 = ((f32[64,128,4]{1,2,0:T(4,128)}), f32[64,128,4]{1,2,0:T(4,128)S(1)}, u32[]{:S(2)}, u32[]{:S(2)}) async-start(f32[64,128,4]{1,2,0:T(4,128)} %broadcast_in_dim.64), calls=%async_computation.1 | async-start | bytes 262144 | tf_op jit(solution)/shard_map/all_to_all | solution.py:34
  41.3 45.6 %all-gather.3.cloned.1.call-done = bf16[8192,128]{0,1:T(8,128)(2,1)} async-done(((bf16[128,128]{0,1:T(8,128)(2,1)}), bf16[8192,128]{0,1:T(8,128)(2,1)}) %all-gather.3.cloned.1.call-update) | async-done | bytes 2097168 | tf_op jit(solution)/shard_map/all_gather | solution.py:44
  86.9 1.7 fusion.40
  88.7 85.9 %while.23 = (s32[]{:T(128)}, f32[128,1,4]{0,2,1:T(4,128)S(1)}, f32[128,1,4]{0,2,1:T(4,128)S(1)}, f32[128,1,4,64]{0,3,2,1:T(8,128)S(1)}, s32[]{:T(128)}, /*index=...) while((s32[]{:T(128)}, f32[128,1,4]{0,2,1:T(4,128)S(1)}, ...), condition=%wide.region_5.6_spmd.clone, body=%wide.region_0.5_spmd.clone.sunk | while | flops 17614608 | bytes 1258975 | solution.py:136
  88.7 0.6 dynamic_slice.68
  89.9 0.8 conditional.3
  92.1 0.8 conditional.3
  92.9 0.6 dynamic_slice.68
  96.9 0.6 dynamic_slice.68
  99.5 0.6 dynamic_slice.68
  103.4 0.6 dynamic_slice.68
  106.1 0.6 dynamic_slice.68
  108.7 0.6 dynamic_slice.68
  111.4 0.6 dynamic_slice.68
  115.3 0.6 dynamic_slice.68
  117.9 0.6 dynamic_slice.68
  120.6 0.6 dynamic_slice.68
  123.2 0.6 dynamic_slice.68
  128.5 0.6 dynamic_slice.68
  136.4 0.6 dynamic_slice.68
  139.0 0.6 dynamic_slice.68
  174.8 0.8 convert_element_type.76
  175.5 4.0 %all-to-all-start.2 = ((bf16[4,32,256]{2,1,0:T(8,128)(2,1)}), bf16[4,32,256]{2,1,0:T(8,128)(2,1)S(1)}, u32[]{:S(2)}, u32[]{:S(2)}) async-start(bf16[4,32,256]{2,1,0:T(8,128)(2,1)} %convert_element_type.76), calls=%async_computation.2 | async-start | bytes 131072 | tf_op jit(solution)/shard_map/all_to_all | solution.py:143
  179.5 5.9 %all-to-all-done.2 = bf16[4,32,256]{2,1,0:T(8,128)(2,1)S(1)} async-done(((bf16[4,32,256]{2,1,0:T(8,128)(2,1)}), bf16[4,32,256]{2,1,0:T(8,128)(2,1)S(1)}, u32[]{:S(2)}, u32[]{:S(2)}) %all-to-all-start.2) | async-done | bytes 65568 | tf_op jit(solution)/shard_map/all_to_all | solution.py:143
  185.5 3.1 %multiply_reduce_fusion.1 = (f32[32]{0:T(128)S(1)}, f32[32,2048]{1,0:T(8,128)S(1)}) fusion(bf16[32,1024]{1,0:T(8,128)(2,1)S(1)} %bitcast.125, bf16[1024,2048]{1,0:T(8,128)(2,1)} %param.23, bf16[32,2048]{1,0:T(8,128)(2,1)S(1)} %copy-done.2), kind=kOutput, calls=%fused_computation.55 | convolution fusion | flops 134610912 | bytes 4653184 | tf_op jit(solution)/shard_map/dot_general | solution.py:144
  188.7 2.0 scatter_custom_fusion
  191.1 51.0 %all_to_all.45 = bf16[64,2,2048]{2,1,0:T(2,128)(2,1)S(1)} all-to-all(bf16[64,2,2048]{2,1,0:T(2,128)(2,1)S(1)} %reshape.375), channel_id=1, replica_groups=mesh['sp'=64,'tp'=4] {'sp'}, dimensions={0} | all-to-all | bytes 1048576 | tf_op jit(solution)/shard_map/all_to_all | solution.py:157
  242.3 3.9 %fusion.25 = f32[128,1024]{1,0:T(8,128)S(1)} fusion(bf16[128,2048]{1,0:T(8,128)(2,1)S(1)} %reshape.376, bf16[1024,6144]{1,0:T(8,128)(2,1)} %all-gather.5.cloned.1.call-done), kind=kOutput, calls=%fused_computation.38 | convolution fusion | flops 536870912 | bytes 5242880 | tf_op jit(solution)/shard_map/erd,edf->erf/dot_general | solution.py:160
  246.1 2.0 copy-done
  248.1 1.5 fusion.30
  249.7 0.6 slice-done
  250.3 0.7 fusion.28
  251.0 0.8 copy.64
  252.4 3.7 %reduce.12 = bf16[128,2048]{1,0:T(8,128)(2,1)S(1)} reduce(bf16[128,1,2048]{2,1,0:T(2,128)(2,1)S(1)} %bitcast.117, bf16[]{:T(256)} %broadcast.238), dimensions={1}, to_apply=%bitcast.108.reduce_sub_computation | reduce | bytes 1048578
  256.1 1.1 reshape.419
  257.2 5.7 %all-to-all-start.4 = ((bf16[64,2,2048]{2,1,0:T(2,128)(2,1)}), bf16[64,2,2048]{2,1,0:T(2,128)(2,1)S(1)}, u32[]{:S(2)}, u32[]{:S(2)}) async-start(bf16[64,2,2048]{2,1,0:T(2,128)(2,1)} %reshape.419), calls=%async_computation.4 | async-start | bytes 1048576 | tf_op jit(solution)/shard_map/all_to_all | solution.py:170
  263.0 17.6 %all-to-all-done.4 = bf16[64,2,2048]{2,1,0:T(2,128)(2,1)S(1)} async-done(((bf16[64,2,2048]{2,1,0:T(2,128)(2,1)}), bf16[64,2,2048]{2,1,0:T(2,128)(2,1)S(1)}, u32[]{:S(2)}, u32[]{:S(2)}) %all-to-all-start.4) | async-done | bytes 524320 | tf_op jit(solution)/shard_map/all_to_all | solution.py:170
  281.5 0.7 gather_fusion
  282.6 0.7 multiply_reduce_fusion
  283.3 0.7 add_convert_fusion
  (247 shorter events, 36.1 us)
Async XLA Ops:
  6.5 4.5 %copy-start.1 = (bf16[1,256,2048]{2,1,0:T(8,128)(2,1)S(1)}, bf16[1,256,2048]{2,1,0:T(8,128)(2,1)}, u32[]{:S(2)}) copy-start(bf16[1,256,2048]{2,1,0:T(8,128)(2,1)} %param.29) | copy-start | bytes 3145732
  6.5 80.4 %all-gather.3.cloned.1.call-start = ((), (), s32[]{:S(2)}) async-start(), calls=%async_computation.5 | async-start | bytes 2129920 | tf_op jit(solution)/shard_map/all_gather | solution.py:44
  8.0 234.3 %all-gather.5.cloned.1.call-start = ((), (), s32[]{:S(2)}) async-start(), calls=%async_computation.6 | async-start | bytes 15728640 | tf_op jit(solution)/shard_map/all_gather | solution.py:18
  11.0 1.8 copy-start.4
  11.1 15.5 %copy-start.3 = (bf16[128,256]{1,0:T(8,128)(2,1)S(1)}, bf16[128,256]{1,0:T(8,128)(2,1)}, u32[]{:S(2)}) copy-start(bf16[128,256]{1,0:T(8,128)(2,1)} %param.17) | copy-start | bytes 196612
  11.1 15.6 %copy-start.6 = (s32[32,2]{0,1:T(2,128)S(1)}, s32[32,2]{0,1:T(2,128)}, u32[]{:S(2)}) copy-start(s32[32,2]{0,1:T(2,128)} %param.25) | copy-start | bytes 772
  11.1 24.8 %copy-start.7 = (f32[128,4]{0,1:T(4,128)S(1)}, f32[128,4]{0,1:T(4,128)}, u32[]{:S(2)}) copy-start(f32[128,4]{0,1:T(4,128)} %param.20) | copy-start | bytes 6148
  13.5 22.4 %all-to-all-start = ((s32[64,1,128]{2,1,0:T(1,128)}), s32[64,1,128]{2,1,0:T(1,128)S(1)}, u32[]{:S(2)}, u32[]{:S(2)}) async-start(s32[64,1,128]{2,1,0:T(1,128)} %broadcast_in_dim.63), calls=%async_computation | async-start | bytes 65536 | tf_op jit(solution)/shard_map/all_to_all | solution.py:34
  36.6 52.0 %all-to-all-start.1 = ((f32[64,128,4]{1,2,0:T(4,128)}), f32[64,128,4]{1,2,0:T(4,128)S(1)}, u32[]{:S(2)}, u32[]{:S(2)}) async-start(f32[64,128,4]{1,2,0:T(4,128)} %broadcast_in_dim.64), calls=%async_computation.1 | async-start | bytes 262144 | tf_op jit(solution)/shard_map/all_to_all | solution.py:34
  88.6 96.9 %copy-start.2 = (bf16[32,2048]{1,0:T(8,128)(2,1)S(1)}, bf16[32,2048]{1,0:T(8,128)(2,1)}, u32[]{:S(2)}) copy-start(bf16[32,2048]{1,0:T(8,128)(2,1)} %param.22) | copy-start | bytes 393220
  174.6 14.0 %copy-start.5 = (f32[2048]{0:T(1024)S(1)}, f32[2048]{0:T(1024)}, u32[]{:S(2)}) copy-start(f32[2048]{0:T(1024)} %param.24) | copy-start | bytes 24580
  175.5 9.9 %all-to-all-start.2 = ((bf16[4,32,256]{2,1,0:T(8,128)(2,1)}), bf16[4,32,256]{2,1,0:T(8,128)(2,1)S(1)}, u32[]{:S(2)}, u32[]{:S(2)}) async-start(bf16[4,32,256]{2,1,0:T(8,128)(2,1)} %convert_element_type.76), calls=%async_computation.2 | async-start | bytes 131072 | tf_op jit(solution)/shard_map/all_to_all | solution.py:143
  242.3 5.8 %copy-start = (bf16[1024,6144]{1,0:T(8,128)(2,1)S(1)}, bf16[1024,6144]{1,0:T(8,128)(2,1)}, u32[]{:S(2)}) copy-start(bf16[1024,6144]{1,0:T(8,128)(2,1)} %all-gather.5.cloned.1.call-done) | copy-start | bytes 37748740
  248.1 2.2 slice-start
  251.0 11.9 %copy-start.8 = (f32[32,2]{0,1:T(2,128)S(1)}, f32[32,2]{0,1:T(2,128)}, u32[]{:S(2)}) copy-start(f32[32,2]{0,1:T(2,128)} %param.26) | copy-start | bytes 772
  257.2 23.4 %all-to-all-start.4 = ((bf16[64,2,2048]{2,1,0:T(2,128)(2,1)}), bf16[64,2,2048]{2,1,0:T(2,128)(2,1)S(1)}, u32[]{:S(2)}, u32[]{:S(2)}) async-start(bf16[64,2,2048]{2,1,0:T(2,128)(2,1)} %reshape.419), calls=%async_computation.4 | async-start | bytes 1048576 | tf_op jit(solution)/shard_map/all_to_all | solution.py:170
Sparse Core Ops, SparseCore 0:
  10.0 76.8 all-gather.2
  88.7 120.2 all-gather.4
where the time goes:
time: 291 us
  waiting for transfers between devices  77.6 us (27%)
  local copies, waits for them, and re-layouts  56.4 us (19%)
  blocking collectives  51 us (18%)
  loops' own time  45.3 us (16%)
  starting transfers between devices  27.4 us (9%)
  between operations  13.8 us (5%)
  matrix products  10.1 us (3%)
  other arithmetic  9.2 us (3%)
    all_to_all x1, blocking collectives, local(): lax.all_to_all(outgoing.reshape(experts, capacity, D), 'sp', split_axis=0...  51 us
    all_gather x1, waiting for transfers between devices, in_one_piece(): out = lax.all_gather(both, axis, axis=dim, tiled=True)  45.6 us
    another operation x1, loops' own time, local(): lax.fori_loop(0, piece_len // block_len, one_block, start_state)  44.1 us
    dynamic_slice x64, local copies, waits for them, and re-layouts, one_block(): lax.dynamic_index_in_dim(doc_all, offset + block_len - 1, 0, keepdims=False)  39 us
    all_to_all x2, starting transfers between devices, from_everyone(): return lax.all_to_all(copies, axis, split_axis=0, concat_axis=0, tiled=True)  17.7 us
    all_to_all x1, waiting for transfers between devices, local(): lax.all_to_all(expert_out, 'sp', split_axis=1, concat_axis=0, tiled=True)  17.6 us
    all_to_all x2, waiting for transfers between devices, from_everyone(): return lax.all_to_all(copies, axis, split_axis=0, concat_axis=0, tiled=True)  8.46 us
    unnamed x27, local copies, waits for them, and re-layouts  7.78 us
  transfers between devices with their start and end apart: 6, of which 4 were waited for; matrix products, arithmetic and copies ran while one was open for 19% of the time, Pallas kernels for 0%

commit v1 on v0

v1 whole, which is shorter than its diff:
```python
import functools

import jax
import jax.numpy as jnp
from jax import lax
from jax.experimental import pallas as pl
from jax.experimental.pallas import tpu as pltpu
from jax.sharding import PartitionSpec as P

MESH = pl.DeviceIdType.MESH
F32, BF16 = jnp.float32, jnp.bfloat16

D = 2048
HEAD_DIM = 64
NZ, NX, NC, NT = 8, 4, 2, 4
PLANE = NX * NC
TOK = 128
HEADS = 4
ROWS = 32
BLK = 144
BACK = 4
WIDE = 256
PIECES = D // WIDE
very_low = -1e30
norm_eps = 1e-06


def at(sp, tp):
    return {"sp": sp, "tp": tp}


def remote(src, dst, send, recv, sp, tp):
    return pltpu.make_async_remote_copy(
        src_ref=src, dst_ref=dst, send_sem=send, recv_sem=recv, device_id=at(sp, tp), device_id_type=MESH
    )


def index_of(z, x, c):
    return ((z + NZ) % NZ * NX + (x + NX) % NX) * NC + (c + NC) % NC


def place():
    sp, tp = lax.axis_index("sp"), lax.axis_index("tp")
    return sp, tp, sp // PLANE, sp // NC % NX, sp % NC


def attention_kernel(
    q_ref, k_ref, v_ref, gate_ref, doc_ref, res_ref, gain_ref, proj_hbm,
    stream_ref, stacked_ref,
    kvg, aux, qs, bias, top, acc, att, planes, proj,
    recv, send, arecv, asend, psem,
):
    sp, tp, z, x, c = place()
    load = pltpu.make_async_copy(proj_hbm, proj, psem)
    load.start()

    barrier = pltpu.get_barrier_semaphore()
    partners = [
        index_of(z + 1, x, c), index_of(z - 1, x, c), index_of(z + 2, x, c), index_of(z - 2, x, c),
        index_of(z, x + 1, c), index_of(z, x + 3, c), index_of(z, x + 2, c), index_of(z, x, c + 1),
        index_of(z + 5, x + 1, c + 1), index_of(z - 5, x + 3, c + 1),
    ]
    for other in partners:
        pl.semaphore_signal(barrier, inc=1, device_id=at(other, tp), device_id_type=MESH)
    for step in range(1, NT):
        pl.semaphore_signal(barrier, inc=1, device_id=at(sp, (tp + step) % NT), device_id_type=MESH)

    kvg[sp, 0:HEAD_DIM, :] = k_ref[...]
    kvg[sp, HEAD_DIM : 2 * HEAD_DIM, :] = v_ref[...]
    aux[...] = jnp.zeros_like(aux)
    aux[0:HEADS, :] = gate_ref[...]
    aux[HEADS : HEADS + 1, :] = doc_ref[...].astype(F32)
    own = aux[...]
    high = own.astype(BF16).astype(F32)
    rest = own - high
    mid = rest.astype(BF16).astype(F32)
    low = rest - mid
    sub = lax.broadcasted_iota(jnp.int32, (8, TOK), 0)
    first = jnp.where(sub < HEADS, high, pltpu.roll(mid, HEADS, 0))
    second = jnp.where(sub < HEADS, low, own)
    kvg[sp, 2 * HEAD_DIM : BLK, :] = jnp.concatenate([first, second], axis=0).astype(BF16)

    lane = lax.broadcasted_iota(jnp.int32, (TOK, TOK), 1)
    for pair in range(HEADS // 2):
        both = q_ref[:, pair * TOK : (pair + 1) * TOK].astype(F32) * (HEAD_DIM**-0.5)
        for half in range(2):
            turned = both if half == 0 else pltpu.roll(both, HEAD_DIM, 1)
            qs[pl.ds((pair * 2 + half) * TOK, TOK), :] = jnp.where(lane < HEAD_DIM, turned, 0.0).astype(BF16)
    query_doc = jnp.broadcast_to(own[HEADS : HEADS + 1, :], (TOK, TOK)).T
    top[...] = jnp.full_like(top, very_low)
    acc[...] = jnp.zeros_like(acc)

    pl.semaphore_wait(barrier, len(partners) + NT - 1)

    def push(slot, target):
        remote(kvg.at[slot], kvg.at[slot], send, recv.at[slot], target, tp).start()

    def arrived(slot):
        remote(kvg.at[slot], kvg.at[slot], send, recv.at[slot], sp, (tp + 1) % NT).wait_recv()

    def spread(slot):
        push(slot, index_of(z, x + 1, c))
        push(slot, index_of(z, x + 3, c))
        push(slot, index_of(z, x + 2, c))
        push(slot, index_of(z, x, c + 1))

    def across(back):
        for step in (1, 3, 2):
            slot = index_of(z - back, x + step, c)
            arrived(slot)
            push(slot, index_of(z, x, c + 1))

    def beside(back):
        for step in range(NX):
            arrived(index_of(z - back, x + step, c + 1))

    extra = index_of(z - 5, x + 3, c + 1)
    extra_off = jnp.where((x == 0) & (c == 0) & (z >= 5), 0.0, -64.0)

    def attend(back):
        plane = (z - back + NZ) % NZ
        slots = [plane * PLANE + k for k in range(PLANE)]
        off = jnp.where(z >= back, 0.0, -64.0)
        offs = [off] * PLANE
        if back == BACK:
            slots.append(extra)
            offs.append(extra_off)
        width = len(slots) * TOK
        gate_first = own[:, 0:1]
        row8 = lax.broadcasted_iota(jnp.int32, (8, TOK), 0)
        blocks = []
        for k, (slot, shift) in enumerate(zip(slots, offs)):
            parts = kvg[slot, 2 * HEAD_DIM : BLK, :].astype(F32)
            upper, lower = parts[0:8], parts[8:16]
            gates = gate_first - (upper + pltpu.roll(upper, HEADS, 0) + lower)
            bias[:, k * TOK : (k + 1) * TOK] = jnp.where(row8 < HEADS, gates, lower + shift)
            blocks.append(kvg[slot, 0 : 2 * HEAD_DIM, :])
        kv = jnp.concatenate(blocks, axis=1)
        row = lax.broadcasted_iota(jnp.int32, kv.shape, 0)
        ones_v = jnp.where(row < HEAD_DIM, jnp.ones_like(kv), kv)
        allowed = jnp.concatenate([query_doc] * len(slots), axis=1) == bias[HEADS : HEADS + 1, 0:width]
        if back == 0:
            key_pos = lax.broadcasted_iota(jnp.int32, (TOK, width), 1)
            query_pos = lax.broadcasted_iota(jnp.int32, (TOK, width), 0) + (x * NC + c) * TOK
            allowed = allowed & (key_pos <= query_pos)
        for head in range(HEADS):
            rows = slice(head * TOK, (head + 1) * TOK)
            scores = jnp.dot(qs[rows, :], kv, preferred_element_type=F32)
            scores = jnp.where(allowed, scores + bias[head : head + 1, 0:width], very_low)
            top_old = top[rows, :]
            top_new = jnp.maximum(top_old, jnp.max(scores, axis=1, keepdims=True))
            weights = jnp.exp(scores - top_new[:, 0:1]).astype(BF16)
            part = lax.dot_general(
                weights, ones_v, (((1,), (1,)), ((), ())), preferred_element_type=F32
            )
            acc[rows, :] = acc[rows, :] * jnp.exp(top_old - top_new) + part
            top[rows, :] = top_new

    one, two, three, four = (index_of(z - back, x, c) for back in (1, 2, 3, 4))
    push(sp, index_of(z + 1, x, c))
    push(sp, index_of(z + 2, x, c))
    spread(sp)
    push(sp, index_of(z + 5, x + 1, c + 1))
    arrived(one)
    spread(one)
    arrived(two)
    push(two, index_of(z + 1, x, c))
    push(two, index_of(z + 2, x, c))
    spread(two)
    across(0)
    across(1)
    beside(0)
    attend(0)
    arrived(three)
    spread(three)
    across(2)
    beside(1)
    attend(1)
    arrived(four)
    spread(four)
    across(3)
    beside(2)
    attend(2)
    across(4)
    beside(3)
    attend(3)
    beside(4)
    arrived(extra)
    attend(4)

    done = []
    for head in range(HEADS):
        summed = acc[head * TOK : (head + 1) * TOK, :]
        done.append(summed / pltpu.roll(summed, HEAD_DIM, 1))
    for pair in range(HEADS // 2):
        left = pltpu.roll(done[2 * pair], HEAD_DIM, 1)
        att[:, pair * TOK : (pair + 1) * TOK] = jnp.where(lane < HEAD_DIM, left, done[2 * pair + 1]).astype(BF16)
    for step in (1, 3, 2):
        other = (tp + step) % NT
        remote(
            att.at[pl.ds(pl.multiple_of(other * ROWS, ROWS), ROWS)], planes.at[tp], asend, arecv.at[tp], sp, other
        ).start()
    load.wait()
    depth = HEADS * HEAD_DIM

    def part_of(rows, group):
        weights = proj[pl.ds(pl.multiple_of(group * depth, depth), depth), :]
        return jnp.dot(rows, weights, preferred_element_type=F32)

    total = part_of(att[pl.ds(pl.multiple_of(tp * ROWS, ROWS), ROWS), :], tp)
    for step in (1, 3, 2):
        other = (tp + step) % NT
        remote(planes.at[other], planes.at[other], asend, arecv.at[other], sp, other).wait_recv()
        total = total + part_of(planes[other], other)
    stream = (res_ref[...].astype(F32) + total).astype(BF16)
    stream_ref[...] = stream
    stream = stream.astype(F32)
    normed = stream * lax.rsqrt(jnp.mean(stream * stream, axis=1, keepdims=True) + norm_eps)
    normed = (normed * gain_ref[...]).astype(BF16)
    for piece in range(PIECES):
        stacked_ref[piece * ROWS : (piece + 1) * ROWS, :] = normed[:, piece * WIDE : (piece + 1) * WIDE]

    count = 5 + 15 + 20
    remote(kvg.at[pl.ds(0, count)], kvg.at[pl.ds(0, count)], send, recv.at[0], sp, (tp + 1) % NT).wait_send()
    remote(planes.at[pl.ds(0, 3)], planes.at[pl.ds(0, 3)], asend, arecv.at[0], sp, (tp + 1) % NT).wait_send()


def expert_kernel(
    stacked_ref, stream_ref, ids_ref, weights_ref, gate_hbm, up_hbm, down_hbm,
    out_ref,
    turn, choose, sent, came, pick, xrows, w_gate, w_up, w_down,
    pieces, half_l, half_r, full_l, full_r, to_r, to_l, back, final,
    wsem, dsend, drecv, ysend, yl, yr, ya, yb, rsend, ra, rb, rl, rr, fsend, frecv,
):
    sp, tp, z, x, c = place()
    own_in_plane = x * NC + c
    right, left, far = (tp + 1) % NT, (tp + 3) % NT, (tp + 2) % NT
    experts = NZ * PLANE
    loads = [
        pltpu.make_async_copy(hbm.at[0], vmem, wsem.at[k])
        for k, (hbm, vmem) in enumerate(((gate_hbm, w_gate), (up_hbm, w_up), (down_hbm, w_down)))
    ]
    for load in loads:
        load.start()

    barrier = pltpu.get_barrier_semaphore()

    def greet(step, carry):
        pl.semaphore_signal(barrier, inc=1, device_id=at((sp + step) % experts, tp), device_id_type=MESH)
        return carry

    lax.fori_loop(1, experts, greet, 0)
    for step in range(1, NT):
        pl.semaphore_signal(barrier, inc=1, device_id=at(sp, (tp + step) % NT), device_id_type=MESH)

    def plane_at(g):
        away = (g + 1) // 2 * (1 - 2 * ((g + 1) % 2))
        return (z + away + NZ) % NZ

    turn[...] = jnp.zeros_like(turn)
    turn[0:2, 0:ROWS] = ids_ref[...].astype(F32)
    turn[2:4, 0:ROWS] = weights_ref[...]
    along = turn[0:8, 0:ROWS]
    columns = turn[...].T[0:ROWS, :]
    low = lax.broadcasted_iota(jnp.int32, (ROWS, ROWS), 0)
    high = lax.broadcasted_iota(jnp.int32, (ROWS, ROWS), 1)
    lane = lax.broadcasted_iota(jnp.int32, (ROWS, 2 * WIDE), 1)
    spread = jnp.where(
        lax.broadcasted_iota(jnp.int32, (ROWS, WIDE), 1) % ROWS == lax.broadcasted_iota(jnp.int32, (ROWS, WIDE), 0),
        1.0, 0.0,
    ).astype(BF16)
    piece_of = (lax.broadcasted_iota(jnp.int32, (8, WIDE), 1) // ROWS).astype(F32)
    targets = []
    for k in range(2):
        line, column = along[k : k + 1, :], columns[:, k : k + 1]
        rank_line = jnp.zeros((1, ROWS), F32)
        rank_column = jnp.zeros((ROWS, 1), F32)
        for other in range(2):
            same = (columns[:, other : other + 1] == line) & (low < high)
            rank_line = rank_line + jnp.sum(jnp.where(same, 1.0, 0.0), axis=0, keepdims=True)
            same = (along[other : other + 1, :] == column) & (high < low)
            rank_column = rank_column + jnp.sum(jnp.where(same, 1.0, 0.0), axis=1, keepdims=True)
        slot = jnp.broadcast_to(line * 2.0 + rank_line, (8, ROWS)).astype(BF16)
        targets.append(jnp.dot(slot, spread, preferred_element_type=F32) * PIECES + piece_of)
        base = (column * 2.0 + rank_column) * PIECES
        for piece in range(PIECES):
            want = (base + piece).astype(jnp.int32)
            for plane in range(NZ):
                spots = lax.broadcasted_iota(jnp.int32, (ROWS, TOK), 1) + plane * TOK
                rows = slice((k * PIECES + piece) * ROWS, (k * PIECES + piece + 1) * ROWS)
                pick[plane, rows, :] = jnp.where(spots == want, 1.0, 0.0).astype(BF16)
    spots = lax.broadcasted_iota(jnp.int32, (experts * 16, WIDE), 0)
    hit = (spots == targets[0][0:1, :].astype(jnp.int32)) | (spots == targets[1][0:1, :].astype(jnp.int32))
    chosen = jnp.where(hit, 1.0, 0.0).astype(BF16)
    sent[...] = (
        jnp.dot(chosen, stacked_ref[...], preferred_element_type=F32).astype(BF16).reshape(experts, 16, WIDE)
    )
    src = lax.broadcasted_iota(jnp.int32, (TOK, TOK), 0)
    dst = lax.broadcasted_iota(jnp.int32, (TOK, TOK), 1)
    choose[0] = jnp.where((dst // 8 == src % 16) & (dst % 8 == src // 16), 1.0, 0.0).astype(BF16)
    choose[1] = jnp.where((src // 8 == dst % 16) & (src % 8 == dst // 16), 1.0, 0.0).astype(BF16)

    pl.semaphore_wait(barrier, experts - 1 + NT - 1)

    def dispatch(g, carry):
        plane = plane_at(g)

        def one(k, inner):
            target = plane * PLANE + k

            @pl.when(target != sp)
            def _():
                remote(sent.at[target], came.at[tp, sp], dsend, drecv.at[z], target, tp).start()

            @pl.when(target == sp)
            def _():
                pltpu.make_async_copy(sent.at[sp], came.at[tp, sp], drecv.at[z]).start()

            return inner

        return lax.fori_loop(0, PLANE, one, carry)

    lax.fori_loop(0, NZ, dispatch, 0)

    def group(ref, source, plane, half=None):
        if half is None:
            return ref.at[source, pl.ds(pl.multiple_of(plane * PLANE, PLANE), PLANE)]
        return ref.at[source, pl.ds(pl.multiple_of(plane * PLANE + half * (PLANE // 2), PLANE // 2), PLANE // 2)]

    def share(g):
        plane = plane_at(g)
        ref = group(came, tp, plane)
        remote(ref, ref, dsend, drecv.at[plane], sp, right).wait_recv()
        remote(ref, ref, ysend, yl.at[g], sp, right).start()
        remote(ref, ref, ysend, yr.at[g], sp, left).start()

    def relay(g):
        plane = plane_at(g)
        ref = group(came, left, plane)
        remote(ref, ref, ysend, yl.at[g], sp, right).wait_recv()
        ref = group(came, left, plane, 0)
        remote(ref, ref, ysend, ya.at[g], sp, right).start()
        ref = group(came, right, plane)
        remote(ref, ref, ysend, yr.at[g], sp, left).wait_recv()
        ref = group(came, right, plane, 1)
        remote(ref, ref, ysend, yb.at[g], sp, left).start()

    def gathered(g):
        plane = plane_at(g)
        ref = group(came, far, plane, 0)
        remote(ref, ref, ysend, ya.at[g], sp, right).wait_recv()
        ref = group(came, far, plane, 1)
        remote(ref, ref, ysend, yb.at[g], sp, right).wait_recv()

    def compute(chunk):
        for k in range(2):
            plane = plane_at(2 * chunk + k)
            for source in range(NT):
                rows = came[source, pl.ds(pl.multiple_of(plane * PLANE, PLANE), PLANE)].reshape(TOK, WIDE)
                ordered = jnp.dot(choose[0], rows, preferred_element_type=F32).astype(BF16)
                q = (k * NT + source) * 16
                for piece in range(PIECES):
                    xrows[q : q + 16, piece * WIDE : (piece + 1) * WIDE] = ordered[piece * 16 : piece * 16 + 16, :]
        rows = xrows[...]
        gate = jnp.dot(rows, w_gate[...], preferred_element_type=F32)
        upper = jnp.dot(rows, w_up[...], preferred_element_type=F32)
        hidden = (gate / (1.0 + jnp.exp(-gate)) * upper).astype(BF16)
        part = jnp.dot(hidden, w_down[...], preferred_element_type=F32).astype(BF16)
        for k in range(2):
            for source in range(NT):
                q = (k * NT + source) * 16
                pieces[2 * chunk + k, source] = part[q : q + 16, :]

    half = D // 2

    def first_halves(g):
        remote(pieces.at[g, far, :, pl.ds(0, half)], half_l.at[g], rsend, ra.at[g], sp, right).start()
        remote(pieces.at[g, far, :, pl.ds(half, half)], half_r.at[g], rsend, rb.at[g], sp, left).start()

    def add_half(g):
        remote(half_l.at[g], half_l.at[g], rsend, ra.at[g], sp, right).wait_recv()
        mine = pieces[g, right]
        to_r[g, :, 0:half] = (mine[:, 0:half].astype(F32) + half_l[g].astype(F32)).astype(BF16)
        to_r[g, :, half:] = mine[:, half:]
        remote(to_r.at[g], full_l.at[g], rsend, rl.at[g], sp, right).start()
        remote(half_r.at[g], half_r.at[g], rsend, rb.at[g], sp, right).wait_recv()
        mine = pieces[g, left]
        to_l[g, :, half:] = (mine[:, half:].astype(F32) + half_r[g].astype(F32)).astype(BF16)
        to_l[g, :, 0:half] = mine[:, 0:half]
        remote(to_l.at[g], full_r.at[g], rsend, rr.at[g], sp, left).start()

    def give_back(g):
        plane = plane_at(g)
        remote(full_l.at[g], full_l.at[g], rsend, rl.at[g], sp, right).wait_recv()
        remote(full_r.at[g], full_r.at[g], rsend, rr.at[g], sp, right).wait_recv()
        total = pieces[g, tp].astype(F32) + full_l[g].astype(F32) + full_r[g].astype(F32)
        total = total.astype(BF16)
        stacked = jnp.concatenate([total[:, k * WIDE : (k + 1) * WIDE] for k in range(PIECES)], axis=0)
        mixed = jnp.dot(choose[1], stacked, preferred_element_type=F32).astype(BF16)
        back[pl.ds(pl.multiple_of(g * PLANE, PLANE), PLANE)] = mixed.reshape(PLANE, 16, WIDE)

        def one(k, carry):
            target = plane * PLANE + k

            @pl.when(target != sp)
            def _():
                remote(back.at[g * PLANE + k], final.at[sp], fsend, frecv.at[z], target, tp).start()

            @pl.when(target == sp)
            def _():
                pltpu.make_async_copy(back.at[g * PLANE + k], final.at[sp], frecv.at[z]).start()

            return carry

        lax.fori_loop(0, PLANE, one, 0)

    chunks = NZ // 2
    share(0)
    share(1)
    for load in loads:
        load.wait()

    def step(chunk, carry):
        relay(2 * chunk)

        @pl.when(chunk < chunks - 1)
        def _():
            share(2 * chunk + 2)

        relay(2 * chunk + 1)

        @pl.when(chunk < chunks - 1)
        def _():
            share(2 * chunk + 3)

        @pl.when(chunk > 0)
        def _():
            add_half(2 * chunk - 2)
            add_half(2 * chunk - 1)

        @pl.when(chunk > 1)
        def _():
            give_back(2 * chunk - 4)
            give_back(2 * chunk - 3)

        gathered(2 * chunk)
        gathered(2 * chunk + 1)
        compute(chunk)
        first_halves(2 * chunk)
        first_halves(2 * chunk + 1)
        return carry

    lax.fori_loop(0, chunks, step, 0)
    give_back(NZ - 4)
    give_back(NZ - 3)
    add_half(NZ - 2)
    add_half(NZ - 1)
    give_back(NZ - 2)
    give_back(NZ - 1)

    def take(g, total):
        plane = plane_at(g)
        ref = final.at[pl.ds(pl.multiple_of(plane * PLANE, PLANE), PLANE)]
        remote(ref, ref, fsend, frecv.at[plane], sp, right).wait_recv()
        rows = final[pl.ds(pl.multiple_of(plane * PLANE, PLANE), PLANE)].reshape(TOK, WIDE)
        return total + jnp.dot(pick[plane], rows, preferred_element_type=F32)

    total = lax.fori_loop(0, NZ, take, jnp.zeros((2 * PIECES * ROWS, WIDE), F32))
    weight0, weight1 = columns[:, 2:3], columns[:, 3:4]
    for piece in range(PIECES):
        lanes = slice(piece * WIDE, (piece + 1) * WIDE)
        one = total[piece * ROWS : (piece + 1) * ROWS]
        two = total[(PIECES + piece) * ROWS : (PIECES + piece + 1) * ROWS]
        out_ref[:, lanes] = (stream_ref[:, lanes].astype(F32) + (weight0 * one + weight1 * two)).astype(BF16)

    some = sent.at[pl.ds(0, experts - 1)]
    remote(some, some, dsend, drecv.at[0], sp, right).wait_send()
    some = came.at[pl.ds(0, 3)]
    remote(some, some, ysend, yl.at[0], sp, right).wait_send()
    some = pieces.at[pl.ds(0, 6)]
    remote(some, some, rsend, ra.at[0], sp, right).wait_send()
    some = final.at[pl.ds(0, experts - 1)]
    remote(some, some, fsend, frecv.at[0], sp, right).wait_send()


def local(
    queries, keys, values, cum_gate, doc_ids, residual, out_proj, norm_gain, route_ids, route_weights,
    expert_gate, expert_up, expert_down,
):
    vmem, anywhere = pl.BlockSpec(memory_space=pltpu.VMEM), pl.BlockSpec(memory_space=pl.ANY)
    dma, sds = pltpu.SemaphoreType.DMA, jax.ShapeDtypeStruct
    experts = NZ * PLANE
    stream, stacked = pl.pallas_call(
        attention_kernel,
        out_shape=(sds((ROWS, D), BF16), sds((PIECES * ROWS, WIDE), BF16)),
        in_specs=[vmem] * 7 + [anywhere],
        out_specs=(vmem, vmem),
        scratch_shapes=[
            pltpu.VMEM((experts, BLK, TOK), BF16),
            pltpu.VMEM((8, TOK), F32),
            pltpu.VMEM((HEADS * TOK, TOK), BF16),
            pltpu.VMEM((8, (PLANE + 1) * TOK), F32),
            pltpu.VMEM((HEADS * TOK, TOK), F32),
            pltpu.VMEM((HEADS * TOK, TOK), F32),
            pltpu.VMEM((TOK, HEADS * HEAD_DIM), BF16),
            pltpu.VMEM((NT, ROWS, HEADS * HEAD_DIM), BF16),
            pltpu.VMEM((NT * HEADS * HEAD_DIM, D), BF16),
            dma((experts,)), dma, dma((NT,)), dma, dma,
        ],
        compiler_params=pltpu.CompilerParams(
            collective_id=0, has_side_effects=True, vmem_limit_bytes=50 << 20
        ),
        name="attention",
    )(queries, keys.T, values.T, cum_gate.T, doc_ids[None], residual, norm_gain[None], out_proj)
    return pl.pallas_call(
        expert_kernel,
        out_shape=sds((ROWS, D), BF16),
        in_specs=[vmem] * 4 + [anywhere] * 3,
        out_specs=vmem,
        scratch_shapes=[
            pltpu.VMEM((TOK, TOK), F32),
            pltpu.VMEM((2, TOK, TOK), BF16),
            pltpu.VMEM((experts, 16, WIDE), BF16),
            pltpu.VMEM((NT, experts, 16, WIDE), BF16),
            pltpu.VMEM((NZ, 2 * PIECES * ROWS, TOK), BF16),
            pltpu.VMEM((TOK, D), BF16),
            pltpu.VMEM((D, WIDE), BF16),
            pltpu.VMEM((D, WIDE), BF16),
            pltpu.VMEM((WIDE, D), BF16),
            pltpu.VMEM((NZ, NT, 16, D), BF16),
            pltpu.VMEM((NZ, 16, D // 2), BF16),
            pltpu.VMEM((NZ, 16, D // 2), BF16),
            pltpu.VMEM((NZ, 16, D), BF16),
            pltpu.VMEM((NZ, 16, D), BF16),
            pltpu.VMEM((NZ, 16, D), BF16),
            pltpu.VMEM((NZ, 16, D), BF16),
            pltpu.VMEM((experts, 16, WIDE), BF16),
            pltpu.VMEM((experts, 16, WIDE), BF16),
            dma((3,)), dma, dma((NZ,)), dma, dma((NZ,)), dma((NZ,)), dma((NZ,)), dma((NZ,)),
            dma, dma((NZ,)), dma((NZ,)), dma((NZ,)), dma((NZ,)), dma, dma((NZ,)),
        ],
        compiler_params=pltpu.CompilerParams(
            collective_id=1, has_side_effects=True, vmem_limit_bytes=50 << 20
        ),
        name="experts",
    )(stacked, stream, route_ids.T, route_weights.T, expert_gate, expert_up, expert_down)


def solution(mesh):
    in_specs = (
        P("sp", "tp"),
        P("sp", "tp"),
        P("sp", "tp"),
        P("sp", "tp"),
        P("sp"),
        P(("sp", "tp"), None),
        P(),
        P(),
        P(("sp", "tp"), None),
        P(("sp", "tp"), None),
        P("sp", None, "tp"),
        P("sp", None, "tp"),
        P("sp", "tp", None),
    )
    out_specs = P(("sp", "tp"), None)
    return jax.shard_map(local, mesh=mesh, in_specs=in_specs, out_specs=out_specs, check_vma=False)
```

time: 291 us -> 101 us (0.35)
  Pallas kernels: 0 us -> 94.6 us
  waiting for transfers between devices: 77.6 us -> 0 us
  blocking collectives: 51 us -> 0 us
  local copies, waits for them, and re-layouts: 56.4 us -> 6.03 us
  loops' own time: 45.3 us -> 0 us
  starting transfers between devices: 27.4 us -> 0 us
  between operations: 13.8 us -> 0.08 us
  matrix products: 10.1 us -> 0 us
  other arithmetic: 9.2 us -> 0 us
    pallas_call x0 -> x2, Pallas kernels: none -> 94.6 us  [the longest x1 60.1 us: local(): pl.pallas_call(expert_kernel, out_shape=sds((ROWS, D), BF16), in_specs=[v...]
    all_to_all x1 -> x0, blocking collectives: 51 us -> none  [local(): lax.all_to_all(outgoing.reshape(experts, capacity, D), 'sp', split_axis=0...]
    all_gather x2 -> x0, waiting for transfers between devices: 45.6 us -> none  [the longest x1 45.6 us: in_one_piece(): out = lax.all_gather(both, axis, axis=dim, tiled=True)]
    another operation x65 -> x0, loops' own time: 45.3 us -> none  [the longest x1 44.1 us: local(): lax.fori_loop(0, piece_len // block_len, one_block, start_state)]
    dynamic_slice x66 -> x0, local copies, waits for them, and re-layouts: 39.1 us -> none  [the longest x64 39 us: one_block(): lax.dynamic_index_in_dim(doc_all, offset + block_len - 1, 0, keepdims=False)]
    all_to_all x4 -> x0, waiting for transfers between devices: 32 us -> none  [the longest x1 17.6 us: local(): lax.all_to_all(expert_out, 'sp', split_axis=1, concat_axis=0, tiled=True)]
    all_to_all x4 -> x0, starting transfers between devices: 27.4 us -> none  [the longest x2 17.7 us: from_everyone(): return lax.all_to_all(copies, axis, split_axis=0, concat_axis=0, tiled=True)]
    dot_general x8 -> x0, matrix products: 10.1 us -> none  [the longest x1 3.85 us: local(): jnp.einsum('erd,edf->erf', arrived, whole_gate, preferred_element_type=jn...]
  transfers between devices with their start and end apart: 6 -> 0, of which waited for: 4 -> 0; matrix products, arithmetic and copies ran while one was open for 19% -> 0% of each run, Pallas kernels for 0% -> 0%
where the time goes in v1:
time: 101 us
  Pallas kernels  94.6 us (94%)
  local copies, waits for them, and re-layouts  6.03 us (6%)
    pallas_call x1, Pallas kernels, local(): pl.pallas_call(expert_kernel, out_shape=sds((ROWS, D), BF16), in_specs=[v...  60.1 us
    pallas_call x1, Pallas kernels, local(): pl.pallas_call(attention_kernel, out_shape=(sds((ROWS, D), BF16), sds((PI...  34.5 us
    unnamed x25, local copies, waits for them, and re-layouts  6.03 us

profile of v1, /device:TPU:1, one launch (start us, length us, event | category | flops | bytes accessed | tf_op | source)
XLA Modules:
  0.0 100.7 jit_solution(12906743496876284460)
XLA Ops:
  0.0 0.0 copy-start.2
  0.0 0.0 copy-start.1
  0.0 0.0 copy-start
  0.0 0.0 copy-start.3
  0.0 1.0 %copy-done.3 = bf16[32,2048]{1,0:T(8,128)(2,1)S(1)} copy-done((bf16[32,2048]{1,0:T(8,128)(2,1)S(1)}, bf16[32,2048]{1,0:T(8,128)(2,1)}, u32[]{:S(2)}) %copy-start.3) | copy-done | bytes 131096
  1.1 0.0 copy-start.4
  1.1 0.8 copy-done.4
  1.9 0.0 copy-start.5
  1.9 0.7 copy-done.5
  2.6 0.0 copy-start.6
  2.6 0.7 copy-done.6
  3.3 0.0 copy-start.7
  3.3 0.7 copy-done.7
  4.0 0.0 copy-start.8
  4.0 0.7 copy-done.8
  4.7 0.0 copy-start.11
  4.7 0.7 copy-done.11
  5.4 0.0 copy-start.9
  5.4 0.0 copy-start.10
  5.4 34.5 %attention.1 = (bf16[32,2048]{1,0:T(8,128)(2,1)S(1)}, bf16[256,256]{1,0:T(8,128)(2,1)S(1)}) custom-call(bf16[128,256]{1,0:T(8,128)(2,1)S(1)} %copy-done.4, bf16[64,128]{1,0:T(8,128)(2,1)S(1)} %bitcast.7, bf16[64,128]{1,0:T(8,128)(2,1)S(1)} %bitcast.8, f32[4,128]{1,0:T(4,128)S(1)} %bitcast.10, s32[1,128]{1,0:T(1,128)S(1)} %bitcast.13, ...), custom_call_target="tpu_custom_call" | custom-call | tf_op jit(solution)/shard_map/attention/pallas_call | solution.py:493
  39.9 0.0 copy-done.2
  39.9 0.0 copy-done.1
  39.9 0.0 copy-done
  39.9 0.0 copy-done.9
  39.9 0.0 copy-done.10
  39.9 60.1 %experts.1 = bf16[32,2048]{1,0:T(8,128)(2,1)S(1)} custom-call(bf16[256,256]{1,0:T(8,128)(2,1)S(1)} %get-tuple-element.7.stacked_ref, bf16[32,2048]{1,0:T(8,128)(2,1)S(1)} %get-tuple-element.8.stream_ref, s32[2,32]{1,0:T(2,128)S(1)} %bitcast.11, f32[2,32]{1,0:T(2,128)S(1)} %bitcast.12, bf16[1,2048,256]{2,1,0:T(8,128)(2,1)S(1)} %copy-done, ...), custom_call_target="tpu_custom_call" | custom-call | tf_op jit(solution)/shard_map/experts/pallas_call | solution.py:515
  100.0 0.7 copy.15
Async XLA Ops:
  0.0 39.9 %copy-start.2 = (bf16[1,256,2048]{2,1,0:T(8,128)(2,1)S(1)}, bf16[1,256,2048]{2,1,0:T(8,128)(2,1)}, u32[]{:S(2)}) copy-start(bf16[1,256,2048]{2,1,0:T(8,128)(2,1)} %down_hbm.1) | copy-start | bytes 3145732
  0.0 39.9 %copy-start.1 = (bf16[1,2048,256]{2,1,0:T(8,128)(2,1)S(1)}, bf16[1,2048,256]{2,1,0:T(8,128)(2,1)}, u32[]{:S(2)}) copy-start(bf16[1,2048,256]{2,1,0:T(8,128)(2,1)} %up_hbm.1) | copy-start | bytes 3145732
  0.0 39.9 %copy-start = (bf16[1,2048,256]{2,1,0:T(8,128)(2,1)S(1)}, bf16[1,2048,256]{2,1,0:T(8,128)(2,1)}, u32[]{:S(2)}) copy-start(bf16[1,2048,256]{2,1,0:T(8,128)(2,1)} %gate_hbm.1) | copy-start | bytes 3145732
  0.0 1.1 %copy-start.3 = (bf16[32,2048]{1,0:T(8,128)(2,1)S(1)}, bf16[32,2048]{1,0:T(8,128)(2,1)}, u32[]{:S(2)}) copy-start(bf16[32,2048]{1,0:T(8,128)(2,1)} %res_ref.1) | copy-start | bytes 393220
  1.1 0.8 copy-start.4
  1.9 0.7 copy-start.5
  2.6 0.7 copy-start.6
  3.3 0.7 copy-start.7
  4.0 0.7 copy-start.8
  4.7 0.7 copy-start.11
  5.4 34.5 %copy-start.9 = (s32[32,2]{0,1:T(2,128)S(1)}, s32[32,2]{0,1:T(2,128)}, u32[]{:S(2)}) copy-start(s32[32,2]{0,1:T(2,128)} %param.21) | copy-start | bytes 772
  5.4 34.6 %copy-start.10 = (f32[32,2]{0,1:T(2,128)S(1)}, f32[32,2]{0,1:T(2,128)}, u32[]{:S(2)}) copy-start(f32[32,2]{0,1:T(2,128)} %param.22) | copy-start | bytes 772

commit v2 on v1

v2 whole, which is shorter than its diff:
```python
import functools

import jax
import jax.numpy as jnp
from jax import lax
from jax.experimental import pallas as pl
from jax.experimental.pallas import tpu as pltpu
from jax.sharding import PartitionSpec as P

MESH = pl.DeviceIdType.MESH
F32, BF16 = jnp.float32, jnp.bfloat16

D = 2048
HEAD_DIM = 64
NZ, NX, NC, NT = 8, 4, 2, 4
PLANE = NX * NC
TOK = 128
HEADS = 4
ROWS = 32
BLK = 144
BACK = 4
WIDE = 256
PIECES = D // WIDE
AHEAD = 4
ORDER = (0, 1, -3, 3, 4, -2, 2, -1)
very_low = -1e30
norm_eps = 1e-06


def at(sp, tp):
    return {"sp": sp, "tp": tp}


def remote(src, dst, send, recv, sp, tp):
    return pltpu.make_async_remote_copy(
        src_ref=src, dst_ref=dst, send_sem=send, recv_sem=recv, device_id=at(sp, tp), device_id_type=MESH
    )


def index_of(z, x, c):
    return ((z + NZ) % NZ * NX + (x + NX) % NX) * NC + (c + NC) % NC


def place():
    sp, tp = lax.axis_index("sp"), lax.axis_index("tp")
    return sp, tp, sp // PLANE, sp // NC % NX, sp % NC


def layer_kernel(
    q_hbm, k_hbm, v_hbm, gates_hbm, doc_hbm, res_hbm, gain_hbm, proj_hbm,
    ids_hbm, weights_hbm, gate_hbm, up_hbm, down_hbm,
    out_ref,
    q_ref, gates_ref, doc_ref, res_ref, gain_ref, ids_ref, weights_ref,
    kvg, aux, qs, bias, top, acc, soft, turned_v, att, planes, proj, kept, stacked,
    turn, chosen, choose, sent, came, pick, xrows, w_gate, w_up, w_down,
    hidden, hid_out, hid_in, pieces, half_l, half_r, full_l, full_r, to_r, to_l, back, final,
    insem, recv, send, arecv, asend, psem,
    wsem, dsend, drecv, ysend, yl, yr, ya, yb, rsend, ra, rb, rl, rr, fsend, frecv,
    gsend, gl, gr, hsend, hrecv,
):
    sp, tp, z, x, c = place()
    right, left, far = (tp + 1) % NT, (tp + 3) % NT, (tp + 2) % NT
    experts = NZ * PLANE
    barrier = pltpu.get_barrier_semaphore()
    in_copies = {}
    for k, (name, hbm, vmem) in enumerate((
        ("k", k_hbm, kvg.at[sp, pl.ds(0, HEAD_DIM)]), ("v", v_hbm, kvg.at[sp, pl.ds(HEAD_DIM, HEAD_DIM)]),
        ("gates", gates_hbm, gates_ref), ("doc", doc_hbm, doc_ref), ("q", q_hbm, q_ref), ("ids", ids_hbm, ids_ref),
        ("weights", weights_hbm, weights_ref), ("res", res_hbm, res_ref), ("gain", gain_hbm, gain_ref),
    )):
        in_copies[name] = pltpu.make_async_copy(hbm, vmem, insem.at[k])
        in_copies[name].start()

    def greet(step, carry):
        pl.semaphore_signal(barrier, inc=1, device_id=at((sp + step) % experts, tp), device_id_type=MESH)
        return carry

    lax.fori_loop(1, experts, greet, 0)
    for step in range(1, NT):
        pl.semaphore_signal(barrier, inc=1, device_id=at(sp, (tp + step) % NT), device_id_type=MESH)
    load = pltpu.make_async_copy(proj_hbm, proj, psem)
    load.start()
    loads = [
        pltpu.make_async_copy(hbm.at[0], vmem, wsem.at[k])
        for k, (hbm, vmem) in enumerate(((down_hbm, w_down.at[tp]), (gate_hbm, w_gate), (up_hbm, w_up)))
    ]
    for load_w in loads:
        load_w.start()
    for name in ("k", "v", "gates", "doc", "q"):
        in_copies[name].wait()

    def part_down(source, part):
        return w_down.at[source, pl.ds(part * (WIDE // 2), WIDE // 2)]

    def share_down():
        loads[0].wait()
        for part in (0, 1):
            ref = part_down(tp, part)
            remote(ref, ref, gsend, gl.at[part], sp, right).start()
            ref = part_down(tp, 1 - part)
            remote(ref, ref, gsend, gr.at[1 - part], sp, left).start()

    def pass_down():
        ref = part_down(left, 0)
        remote(ref, ref, gsend, gl.at[0], sp, right).wait_recv()
        remote(ref, ref, gsend, gl.at[2], sp, right).start()
        ref = part_down(right, 1)
        remote(ref, ref, gsend, gr.at[1], sp, right).wait_recv()
        remote(ref, ref, gsend, gr.at[2], sp, left).start()

    def all_down():
        for source, part, sem in ((left, 1, gl.at[1]), (right, 0, gr.at[0]), (far, 0, gl.at[2]), (far, 1, gr.at[2])):
            ref = part_down(source, part)
            remote(ref, ref, gsend, sem, sp, right).wait_recv()

    aux[...] = jnp.zeros_like(aux)
    aux[0:HEADS, :] = gates_ref[...]
    aux[HEADS : HEADS + 1, :] = doc_ref[...].astype(F32)
    own = aux[...]
    high = own.astype(BF16).astype(F32)
    rest = own - high
    mid = rest.astype(BF16).astype(F32)
    low = rest - mid
    sub = lax.broadcasted_iota(jnp.int32, (8, TOK), 0)
    first = jnp.where(sub < HEADS, high, pltpu.roll(mid, HEADS, 0))
    second = jnp.where(sub < HEADS, low, own)
    kvg[sp, 2 * HEAD_DIM : BLK, :] = jnp.concatenate([first, second], axis=0).astype(BF16)

    lane = lax.broadcasted_iota(jnp.int32, (TOK, TOK), 1)
    for pair in range(HEADS // 2):
        both = q_ref[:, pair * TOK : (pair + 1) * TOK].astype(F32) * (HEAD_DIM**-0.5)
        for half in range(2):
            turned = both if half == 0 else pltpu.roll(both, HEAD_DIM, 1)
            qs[pl.ds((pair * 2 + half) * TOK, TOK), :] = jnp.where(lane < HEAD_DIM, turned, 0.0).astype(BF16)
    query_doc = jnp.broadcast_to(own[HEADS : HEADS + 1, :], (TOK, TOK)).T
    top[...] = jnp.full_like(top, very_low)
    acc[...] = jnp.zeros_like(acc)

    with jax.named_scope("barrier"):
        pl.semaphore_wait(barrier, experts - 1 + NT - 1)

    def plane_at(g):
        return (z + ORDER[g] + NZ) % NZ

    def prepare():
        in_copies["ids"].wait()
        in_copies["weights"].wait()
        turn[...] = jnp.zeros_like(turn)
        turn[0:2, 0:ROWS] = ids_ref[...].astype(F32)
        turn[2:4, 0:ROWS] = weights_ref[...]
        along = turn[0:8, 0:ROWS]
        columns = turn[...].T[0:ROWS, :]
        low = lax.broadcasted_iota(jnp.int32, (ROWS, ROWS), 0)
        high = lax.broadcasted_iota(jnp.int32, (ROWS, ROWS), 1)
        lane = lax.broadcasted_iota(jnp.int32, (ROWS, 2 * WIDE), 1)
        spread = jnp.where(
            lax.broadcasted_iota(jnp.int32, (ROWS, WIDE), 1) % ROWS == lax.broadcasted_iota(jnp.int32, (ROWS, WIDE), 0),
            1.0, 0.0,
        ).astype(BF16)
        piece_of = (lax.broadcasted_iota(jnp.int32, (8, WIDE), 1) // ROWS).astype(F32)
        targets = []
        for k in range(2):
            line, column = along[k : k + 1, :], columns[:, k : k + 1]
            rank_line = jnp.zeros((1, ROWS), F32)
            rank_column = jnp.zeros((ROWS, 1), F32)
            for other in range(2):
                same = (columns[:, other : other + 1] == line) & (low < high)
                rank_line = rank_line + jnp.sum(jnp.where(same, 1.0, 0.0), axis=0, keepdims=True)
                same = (along[other : other + 1, :] == column) & (high < low)
                rank_column = rank_column + jnp.sum(jnp.where(same, 1.0, 0.0), axis=1, keepdims=True)
            slot = jnp.broadcast_to(line * 2.0 + rank_line, (8, ROWS)).astype(BF16)
            targets.append(jnp.dot(slot, spread, preferred_element_type=F32) * PIECES + piece_of)
            base = (column * 2.0 + rank_column) * PIECES
            for piece in range(PIECES):
                want = (base + piece).astype(jnp.int32)
                for plane in range(NZ):
                    spots = lax.broadcasted_iota(jnp.int32, (ROWS, TOK), 1) + plane * TOK
                    rows = slice((k * PIECES + piece) * ROWS, (k * PIECES + piece + 1) * ROWS)
                    pick[plane, rows, :] = jnp.where(spots == want, 1.0, 0.0).astype(BF16)
        spots = lax.broadcasted_iota(jnp.int32, (experts * 16, WIDE), 0)
        hit = (spots == targets[0][0:1, :].astype(jnp.int32)) | (spots == targets[1][0:1, :].astype(jnp.int32))
        chosen[...] = jnp.where(hit, 1.0, 0.0).astype(BF16)
        src = lax.broadcasted_iota(jnp.int32, (TOK, TOK), 0)
        dst = lax.broadcasted_iota(jnp.int32, (TOK, TOK), 1)
        choose[0] = jnp.where((dst // 8 == src % 16) & (dst % 8 == src // 16), 1.0, 0.0).astype(BF16)
        choose[1] = jnp.where((src // 8 == dst % 16) & (src % 8 == dst // 16), 1.0, 0.0).astype(BF16)

    def push(slot, target):
        remote(kvg.at[slot], kvg.at[slot], send, recv.at[slot], target, tp).start()

    def arrived(slot):
        remote(kvg.at[slot], kvg.at[slot], send, recv.at[slot], sp, (tp + 1) % NT).wait_recv()

    def spread(slot):
        push(slot, index_of(z, x + 1, c))
        push(slot, index_of(z, x + 3, c))
        push(slot, index_of(z, x + 2, c))
        push(slot, index_of(z, x, c + 1))

    def across(back):
        for step in (1, 3, 2):
            slot = index_of(z - back, x + step, c)
            arrived(slot)
            push(slot, index_of(z, x, c + 1))

    def beside(back):
        for step in range(NX):
            arrived(index_of(z - back, x + step, c + 1))

    extra = index_of(z - 5, x + 3, c + 1)
    extra_off = jnp.where((x == 0) & (c == 0) & (z >= 5), 0.0, -64.0)

    def attend(back):
        plane = (z - back + NZ) % NZ
        slots = [plane * PLANE + k for k in range(PLANE)]
        off = jnp.where(z >= back, 0.0, -64.0)
        offs = [off] * PLANE
        if back == BACK:
            slots.append(extra)
            offs.append(extra_off)
        width = len(slots) * TOK
        gate_first = own[:, 0:1]
        row8 = lax.broadcasted_iota(jnp.int32, (8, TOK), 0)
        blocks = []
        for k, (slot, shift) in enumerate(zip(slots, offs)):
            parts = kvg[slot, 2 * HEAD_DIM : BLK, :].astype(F32)
            upper, lower = parts[0:8], parts[8:16]
            gates = gate_first - (upper + pltpu.roll(upper, HEADS, 0) + lower)
            bias[:, k * TOK : (k + 1) * TOK] = jnp.where(row8 < HEADS, gates, lower + shift)
            blocks.append(kvg[slot, 0 : 2 * HEAD_DIM, :])
        kv = jnp.concatenate(blocks, axis=1)
        row = lax.broadcasted_iota(jnp.int32, kv.shape, 0)
        turned_v[0:width, :] = jnp.where(row < HEAD_DIM, jnp.ones_like(kv), kv).T
        allowed = jnp.concatenate([query_doc] * len(slots), axis=1) == bias[HEADS : HEADS + 1, 0:width]
        if back == 0:
            key_pos = lax.broadcasted_iota(jnp.int32, (TOK, width), 1)
            query_pos = lax.broadcasted_iota(jnp.int32, (TOK, width), 0) + (x * NC + c) * TOK
            allowed = allowed & (key_pos <= query_pos)
        for head in range(HEADS):
            rows = slice(head * TOK, (head + 1) * TOK)
            scores = jnp.dot(qs[rows, :], kv, preferred_element_type=F32)
            scores = jnp.where(allowed, scores + bias[head : head + 1, 0:width], very_low)
            top_old = top[rows, :]
            top_new = jnp.maximum(top_old, jnp.max(scores, axis=1, keepdims=True))
            soft[rows, 0:width] = jnp.exp(scores - top_new[:, 0:1]).astype(BF16)
            acc[rows, :] = acc[rows, :] * jnp.exp(top_old - top_new)
            top[rows, :] = top_new
        acc[...] += jnp.dot(soft[:, 0:width], turned_v[0:width, :], preferred_element_type=F32)

    one, two, three, four = (index_of(z - back, x, c) for back in (1, 2, 3, 4))
    push(sp, index_of(z + 1, x, c))
    push(sp, index_of(z + 2, x, c))
    spread(sp)
    push(sp, index_of(z + 5, x + 1, c + 1))

    @pl.when(c == 0)
    def _():
        share_down()

    with jax.named_scope("prepare"):
        prepare()
    with jax.named_scope("w_one"):
        arrived(one)
    spread(one)
    with jax.named_scope("w_two"):
        arrived(two)
    push(two, index_of(z + 1, x, c))
    push(two, index_of(z + 2, x, c))
    spread(two)
    with jax.named_scope("w_across0"):
        across(0)
    with jax.named_scope("w_beside0"):
        beside(0)
    with jax.named_scope("attend0"):
        attend(0)
    with jax.named_scope("w_across1"):
        across(1)
    with jax.named_scope("w_three"):
        arrived(three)
    spread(three)
    with jax.named_scope("w_beside1"):
        beside(1)
    with jax.named_scope("attend1"):
        attend(1)
    with jax.named_scope("w_four"):
        arrived(four)
    spread(four)

    @pl.when(c == 0)
    def _():
        with jax.named_scope("pass_down"):
            pass_down()

    with jax.named_scope("w_across2"):
        across(2)
    with jax.named_scope("w_across3"):
        across(3)
    with jax.named_scope("w_beside2"):
        beside(2)
    with jax.named_scope("attend2"):
        attend(2)

    with jax.named_scope("w_across4"):
        across(4)
    with jax.named_scope("w_beside3"):
        beside(3)
    with jax.named_scope("attend3"):
        attend(3)
    with jax.named_scope("w_beside4"):
        beside(4)
    with jax.named_scope("w_extra"):
        arrived(extra)
    with jax.named_scope("attend4"):
        attend(4)

    with jax.named_scope("project"):
        done = []
        for head in range(HEADS):
            summed = acc[head * TOK : (head + 1) * TOK, :]
            done.append(summed / pltpu.roll(summed, HEAD_DIM, 1))
        for pair in range(HEADS // 2):
            moved = pltpu.roll(done[2 * pair], HEAD_DIM, 1)
            att[:, pair * TOK : (pair + 1) * TOK] = jnp.where(lane < HEAD_DIM, moved, done[2 * pair + 1]).astype(BF16)
        for step in (1, 3, 2):
            other = (tp + step) % NT
            remote(
                att.at[pl.ds(pl.multiple_of(other * ROWS, ROWS), ROWS)], planes.at[tp], asend, arecv.at[tp], sp, other
            ).start()
        load.wait()
        in_copies["res"].wait()
        in_copies["gain"].wait()
        depth = HEADS * HEAD_DIM

        def part_of(rows, group):
            weights = proj[pl.ds(pl.multiple_of(group * depth, depth), depth), :]
            return jnp.dot(rows, weights, preferred_element_type=F32)

        total = part_of(att[pl.ds(pl.multiple_of(tp * ROWS, ROWS), ROWS), :], tp)
        for step in (1, 3, 2):
            other = (tp + step) % NT
            remote(planes.at[other], planes.at[other], asend, arecv.at[other], sp, other).wait_recv()
            total = total + part_of(planes[other], other)
        stream = (res_ref[...].astype(F32) + total).astype(BF16)
        kept[...] = stream
        stream = stream.astype(F32)
        normed = stream * lax.rsqrt(jnp.mean(stream * stream, axis=1, keepdims=True) + norm_eps)
        normed = (normed * gain_ref[...]).astype(BF16)
        for piece in range(PIECES):
            stacked[piece * ROWS : (piece + 1) * ROWS, :] = normed[:, piece * WIDE : (piece + 1) * WIDE]

    for g in range(NZ):
        plane = (z - ORDER[g] + NZ) % NZ
        rows = pl.ds(pl.multiple_of(plane * TOK, TOK), TOK)
        picked = jnp.dot(chosen[rows, :], stacked[...], preferred_element_type=F32).astype(BF16)
        sent[pl.ds(pl.multiple_of(plane * PLANE, PLANE), PLANE)] = picked.reshape(PLANE, 16, WIDE)

        def one_row(k, carry, plane=plane):
            target = plane * PLANE + k
            remote(sent.at[target], came.at[tp, sp], dsend, drecv.at[z], target, tp).start()
            return carry

        if ORDER[g] == 0:
            for step in range(1, PLANE):
                target = plane * PLANE + (x * NC + c + step) % PLANE
                remote(sent.at[target], came.at[tp, sp], dsend, drecv.at[z], target, tp).start()
            pltpu.make_async_copy(sent.at[sp], came.at[tp, sp], drecv.at[z]).start()
        else:
            lax.fori_loop(0, PLANE, one_row, 0)

    def group(ref, source, plane, half=None):
        if half is None:
            return ref.at[source, pl.ds(pl.multiple_of(plane * PLANE, PLANE), PLANE)]
        return ref.at[source, pl.ds(pl.multiple_of(plane * PLANE + half * (PLANE // 2), PLANE // 2), PLANE // 2)]

    def share(g):
        plane = plane_at(g)
        ref = group(came, tp, plane)
        remote(ref, ref, dsend, drecv.at[plane], sp, right).wait_recv()
        remote(ref, ref, ysend, yl.at[g], sp, right).start()
        remote(ref, ref, ysend, yr.at[g], sp, left).start()

    def relay(g):
        plane = plane_at(g)
        ref = group(came, left, plane)
        remote(ref, ref, ysend, yl.at[g], sp, right).wait_recv()
        ref = group(came, left, plane, 0)
        remote(ref, ref, ysend, ya.at[g], sp, right).start()
        ref = group(came, right, plane)
        remote(ref, ref, ysend, yr.at[g], sp, left).wait_recv()
        ref = group(came, right, plane, 1)
        remote(ref, ref, ysend, yb.at[g], sp, left).start()

    def gathered(g):
        plane = plane_at(g)
        ref = group(came, far, plane, 0)
        remote(ref, ref, ysend, ya.at[g], sp, right).wait_recv()
        ref = group(came, far, plane, 1)
        remote(ref, ref, ysend, yb.at[g], sp, right).wait_recv()

    def compute(chunk):
        for k in range(2):
            plane = plane_at(2 * chunk + k)
            for source in range(NT):
                rows = came[source, pl.ds(pl.multiple_of(plane * PLANE, PLANE), PLANE)].reshape(TOK, WIDE)
                ordered = jnp.dot(choose[0], rows, preferred_element_type=F32).astype(BF16)
                q = (k * NT + source) * 16
                for piece in range(PIECES):
                    xrows[q : q + 16, piece * WIDE : (piece + 1) * WIDE] = ordered[piece * 16 : piece * 16 + 16, :]
        rows = xrows[...]
        gate = jnp.dot(rows, w_gate[...], preferred_element_type=F32)
        upper = jnp.dot(rows, w_up[...], preferred_element_type=F32)
        hidden[...] = (gate / (1.0 + jnp.exp(-gate)) * upper).astype(BF16)

    def multiply(chunk):
        part = jnp.dot(hidden[...], w_down[tp], preferred_element_type=F32).astype(BF16)
        for k in range(2):
            for source in range(NT):
                q = (k * NT + source) * 16
                pieces[2 * chunk + k, source] = part[q : q + 16, :]

    def send_hidden(chunk):
        for k in range(2):
            g = 2 * chunk + k
            for source in range(NT):
                q = (k * NT + source) * 16
                hid_out[g, source] = hidden[q : q + 16, :]
            hid_in[g, tp] = hid_out[g, tp]
            for other in (right, left, far):
                remote(hid_out.at[g, other], hid_in.at[g, tp], hsend, hrecv.at[g], sp, other).start()

    def finish(chunk):
        for k in range(2):
            g = 2 * chunk + k
            some = hid_in.at[g, pl.ds(0, NT - 1)]
            remote(some, some, hsend, hrecv.at[g], sp, right).wait_recv()
        total = jnp.zeros((32, D), F32)
        for source in range(NT):
            rows = hid_in[2 * chunk : 2 * chunk + 2, source].reshape(32, WIDE)
            total = total + jnp.dot(rows, w_down[source], preferred_element_type=F32)
        total = total.astype(BF16)
        for k in range(2):
            hand_back(2 * chunk + k, total[16 * k : 16 * k + 16, :])

    half = D // 2

    def first_halves(g):
        remote(pieces.at[g, far, :, pl.ds(0, half)], half_l.at[g], rsend, ra.at[g], sp, right).start()
        remote(pieces.at[g, far, :, pl.ds(half, half)], half_r.at[g], rsend, rb.at[g], sp, left).start()

    def add_half(g):
        remote(half_l.at[g], half_l.at[g], rsend, ra.at[g], sp, right).wait_recv()
        mine = pieces[g, right]
        to_r[g, :, 0:half] = (mine[:, 0:half].astype(F32) + half_l[g].astype(F32)).astype(BF16)
        to_r[g, :, half:] = mine[:, half:]
        remote(to_r.at[g], full_l.at[g], rsend, rl.at[g], sp, right).start()
        remote(half_r.at[g], half_r.at[g], rsend, rb.at[g], sp, right).wait_recv()
        mine = pieces[g, left]
        to_l[g, :, half:] = (mine[:, half:].astype(F32) + half_r[g].astype(F32)).astype(BF16)
        to_l[g, :, 0:half] = mine[:, 0:half]
        remote(to_l.at[g], full_r.at[g], rsend, rr.at[g], sp, left).start()

    def give_back(g):
        plane = plane_at(g)
        remote(full_l.at[g], full_l.at[g], rsend, rl.at[g], sp, right).wait_recv()
        remote(full_r.at[g], full_r.at[g], rsend, rr.at[g], sp, right).wait_recv()
        total = pieces[g, tp].astype(F32) + full_l[g].astype(F32) + full_r[g].astype(F32)
        hand_back(g, total.astype(BF16))

    def hand_back(g, total):
        plane = plane_at(g)
        stacked = jnp.concatenate([total[:, k * WIDE : (k + 1) * WIDE] for k in range(PIECES)], axis=0)
        mixed = jnp.dot(choose[1], stacked, preferred_element_type=F32).astype(BF16)
        back[pl.ds(pl.multiple_of(g * PLANE, PLANE), PLANE)] = mixed.reshape(PLANE, 16, WIDE)

        def one_row(k, carry):
            target = plane * PLANE + k
            remote(back.at[g * PLANE + k], final.at[sp], fsend, frecv.at[z], target, tp).start()
            return carry

        if ORDER[g] == 0:
            own = x * NC + c
            for step in range(1, PLANE):
                k = (own + step) % PLANE
                remote(
                    back.at[g * PLANE + k], final.at[sp], fsend, frecv.at[z], plane * PLANE + k, tp
                ).start()
            pltpu.make_async_copy(back.at[g * PLANE + own], final.at[sp], frecv.at[z]).start()
        else:
            lax.fori_loop(0, PLANE, one_row, 0)

    chunks = NZ // 2
    for g in range(AHEAD):
        with jax.named_scope(f"share{g}"):
            share(g)
    for g in range(AHEAD, NZ):
        with jax.named_scope(f"relay{g - AHEAD}"):
            relay(g - AHEAD)
        with jax.named_scope(f"share{g}"):
            share(g)
    for load_w in loads[1:]:
        load_w.wait()

    @pl.when(c == 1)
    def _():
        loads[0].wait()


    def first_return(chunk):
        @pl.when(c == 1)
        def _():
            for g in (2 * chunk, 2 * chunk + 1):
                with jax.named_scope(f"add_half{g}"):
                    add_half(g)

    def last_return(chunk):
        @pl.when(c == 0)
        def _():
            if chunk == 0:
                with jax.named_scope("all_down"):
                    all_down()
            with jax.named_scope(f"finish{chunk}"):
                finish(chunk)

        @pl.when(c == 1)
        def _():
            for g in (2 * chunk, 2 * chunk + 1):
                with jax.named_scope(f"back{g}"):
                    give_back(g)

    for chunk in range(chunks):
        for g in (2 * chunk, 2 * chunk + 1):
            with jax.named_scope(f"gathered{g}"):
                gathered(g)
        with jax.named_scope(f"compute{chunk}"):
            compute(chunk)

        @pl.when(c == 0)
        def _(chunk=chunk):
            send_hidden(chunk)

        @pl.when(c == 1)
        def _(chunk=chunk):
            with jax.named_scope(f"multiply{chunk}"):
                multiply(chunk)
            first_halves(2 * chunk)
            first_halves(2 * chunk + 1)

        if chunk < 2:
            for g in (2 * chunk + AHEAD, 2 * chunk + AHEAD + 1):
                with jax.named_scope(f"relay{g}"):
                    relay(g)
        if chunk > 0:
            first_return(chunk - 1)
        if chunk > 1:
            last_return(chunk - 2)
    last_return(chunks - 2)
    first_return(chunks - 1)
    last_return(chunks - 1)

    total = jnp.zeros((2 * PIECES * ROWS, WIDE), F32)
    for g in range(NZ):
        plane = (z - ORDER[g] + NZ) % NZ
        ref = final.at[pl.ds(pl.multiple_of(plane * PLANE, PLANE), PLANE)]
        with jax.named_scope(f"take{g}"):
            remote(ref, ref, fsend, frecv.at[plane], sp, right).wait_recv()
        rows = final[pl.ds(pl.multiple_of(plane * PLANE, PLANE), PLANE)].reshape(TOK, WIDE)
        total = total + jnp.dot(pick[plane], rows, preferred_element_type=F32)
    columns = turn[...].T[0:ROWS, :]
    weight0, weight1 = columns[:, 2:3], columns[:, 3:4]
    for piece in range(PIECES):
        lanes = slice(piece * WIDE, (piece + 1) * WIDE)
        one = total[piece * ROWS : (piece + 1) * ROWS]
        two = total[(PIECES + piece) * ROWS : (PIECES + piece + 1) * ROWS]
        out_ref[:, lanes] = (kept[:, lanes].astype(F32) + (weight0 * one + weight1 * two)).astype(BF16)

    some = sent.at[pl.ds(0, experts - 1)]
    remote(some, some, dsend, drecv.at[0], sp, right).wait_send()
    some = came.at[pl.ds(0, 3)]
    remote(some, some, ysend, yl.at[0], sp, right).wait_send()

    @pl.when(c == 0)
    def _():
        some = w_down.at[pl.ds(0, 3)]
        remote(some, some, gsend, gl.at[0], sp, right).wait_send()
        some = hid_in.at[pl.ds(0, 6)]
        remote(some, some, hsend, hrecv.at[0], sp, right).wait_send()

    @pl.when(c == 1)
    def _():
        some = pieces.at[pl.ds(0, 6)]
        remote(some, some, rsend, ra.at[0], sp, right).wait_send()

    some = final.at[pl.ds(0, experts - 1)]
    remote(some, some, fsend, frecv.at[0], sp, right).wait_send()

    count = 5 + 15 + 20
    remote(kvg.at[pl.ds(0, count)], kvg.at[pl.ds(0, count)], send, recv.at[0], sp, (tp + 1) % NT).wait_send()
    remote(planes.at[pl.ds(0, 3)], planes.at[pl.ds(0, 3)], asend, arecv.at[0], sp, (tp + 1) % NT).wait_send()


def local(
    queries, keys, values, cum_gate, doc_ids, residual, out_proj, norm_gain, route_ids, route_weights,
    expert_gate, expert_up, expert_down,
):
    anywhere = pl.BlockSpec(memory_space=pl.ANY)
    dma, experts = pltpu.SemaphoreType.DMA, NZ * PLANE
    wide_heads = HEADS * HEAD_DIM
    return pl.pallas_call(
        layer_kernel,
        out_shape=jax.ShapeDtypeStruct((ROWS, D), BF16),
        in_specs=[anywhere] * 13,
        out_specs=pl.BlockSpec(memory_space=pltpu.VMEM),
        scratch_shapes=[
            pltpu.VMEM((TOK, wide_heads), BF16),
            pltpu.VMEM((HEADS, TOK), F32),
            pltpu.VMEM((1, TOK), jnp.int32),
            pltpu.VMEM((ROWS, D), BF16),
            pltpu.VMEM((1, D), F32),
            pltpu.VMEM((2, ROWS), jnp.int32),
            pltpu.VMEM((2, ROWS), F32),
            pltpu.VMEM((experts, BLK, TOK), BF16),
            pltpu.VMEM((8, TOK), F32),
            pltpu.VMEM((HEADS * TOK, TOK), BF16),
            pltpu.VMEM((8, (PLANE + 1) * TOK), F32),
            pltpu.VMEM((HEADS * TOK, TOK), F32),
            pltpu.VMEM((HEADS * TOK, TOK), F32),
            pltpu.VMEM((HEADS * TOK, (PLANE + 1) * TOK), BF16),
            pltpu.VMEM(((PLANE + 1) * TOK, TOK), BF16),
            pltpu.VMEM((TOK, wide_heads), BF16),
            pltpu.VMEM((NT, ROWS, wide_heads), BF16),
            pltpu.VMEM((NT * wide_heads, D), BF16),
            pltpu.VMEM((ROWS, D), BF16),
            pltpu.VMEM((PIECES * ROWS, WIDE), BF16),
            pltpu.VMEM((TOK, TOK), F32),
            pltpu.VMEM((experts * 16, WIDE), BF16),
            pltpu.VMEM((2, TOK, TOK), BF16),
            pltpu.VMEM((experts, 16, WIDE), BF16),
            pltpu.VMEM((NT, experts, 16, WIDE), BF16),
            pltpu.VMEM((NZ, 2 * PIECES * ROWS, TOK), BF16),
            pltpu.VMEM((TOK, D), BF16),
            pltpu.VMEM((D, WIDE), BF16),
            pltpu.VMEM((D, WIDE), BF16),
            pltpu.VMEM((NT, WIDE, D), BF16),
            pltpu.VMEM((TOK, WIDE), BF16),
            pltpu.VMEM((NZ, NT, 16, WIDE), BF16),
            pltpu.VMEM((NZ, NT, 16, WIDE), BF16),
            pltpu.VMEM((NZ, NT, 16, D), BF16),
            pltpu.VMEM((NZ, 16, D // 2), BF16),
            pltpu.VMEM((NZ, 16, D // 2), BF16),
            pltpu.VMEM((NZ, 16, D), BF16),
            pltpu.VMEM((NZ, 16, D), BF16),
            pltpu.VMEM((NZ, 16, D), BF16),
            pltpu.VMEM((NZ, 16, D), BF16),
            pltpu.VMEM((experts, 16, WIDE), BF16),
            pltpu.VMEM((experts, 16, WIDE), BF16),
            dma((9,)), dma((experts,)), dma, dma((NT,)), dma, dma,
            dma((3,)), dma, dma((NZ,)), dma, dma((NZ,)), dma((NZ,)), dma((NZ,)), dma((NZ,)),
            dma, dma((NZ,)), dma((NZ,)), dma((NZ,)), dma((NZ,)), dma, dma((NZ,)),
            dma, dma((3,)), dma((3,)), dma, dma((NZ,)),
        ],
        compiler_params=pltpu.CompilerParams(
            collective_id=0, has_side_effects=True, vmem_limit_bytes=60 << 20
        ),
        name="layer",
    )(
        queries, keys.T, values.T, cum_gate.T, doc_ids[None], residual, norm_gain[None], out_proj,
        route_ids.T, route_weights.T, expert_gate, expert_up, expert_down,
    )


def solution(mesh):
    in_specs = (
        P("sp", "tp"),
        P("sp", "tp"),
        P("sp", "tp"),
        P("sp", "tp"),
        P("sp"),
        P(("sp", "tp"), None),
        P(),
        P(),
        P(("sp", "tp"), None),
        P(("sp", "tp"), None),
        P("sp", None, "tp"),
        P("sp", None, "tp"),
        P("sp", "tp", None),
    )
    out_specs = P(("sp", "tp"), None)
    return jax.shard_map(local, mesh=mesh, in_specs=in_specs, out_specs=out_specs, check_vma=False)
```

time: 101 us -> 84.6 us (0.84)
  Pallas kernels: 94.6 us -> 83 us
  local copies, waits for them, and re-layouts: 6.03 us -> 1.57 us
    pallas_call x2 -> x1, Pallas kernels: 94.6 us -> 83 us  [local(): pl.pallas_call(layer_kernel, out_shape=jax.ShapeDtypeStruct((ROWS, D), BF...]
    unnamed x25 -> x1, local copies, waits for them, and re-layouts: 6.03 us -> 1.57 us
where the time goes in v2:
time: 84.6 us
  Pallas kernels  83 us (98%)
  local copies, waits for them, and re-layouts  1.57 us (2%)
    pallas_call x1, Pallas kernels, local(): pl.pallas_call(layer_kernel, out_shape=jax.ShapeDtypeStruct((ROWS, D), BF...  83 us

profile of v2, /device:TPU:1, one launch (start us, length us, event | category | flops | bytes accessed | tf_op | source)
XLA Modules:
  0.0 84.6 jit_solution(15512570471543577885)
XLA Ops:
  0.0 83.0 %layer.1 = bf16[32,2048]{1,0:T(8,128)(2,1)} custom-call(bf16[128,256]{1,0:T(8,128)(2,1)} %q_hbm.1, bf16[64,128]{1,0:T(8,128)(2,1)} %bitcast.7, bf16[64,128]{1,0:T(8,128)(2,1)} %bitcast.8, f32[4,128]{1,0:T(4,128)} %bitcast.10, s32[1,128]{1,0:T(1,128)} %bitcast.13, bf16[32,2048]{1,0:T(8,128)(2,1)} %res_hbm.1, f32[1,2048]{1,0:T(1,128)} %bitcast.9, ...), custom_call_target="tpu_custom_call" | custom-call | tf_op jit(solution)/shard_map/layer/pallas_call | solution.py:608
  83.0 1.6 %copy.15 = bf16[32,2048]{1,0:T(8,128)(2,1)} copy(bf16[32,2048]{1,0:T(8,128)(2,1)} %layer.1) | data formatting | bytes 262144

commit v3 on v2

--- a/solution.py
+++ b/solution.py
@@ -21,8 +21,7 @@
 BACK = 4
 WIDE = 256
 PIECES = D // WIDE
-AHEAD = 4
-ORDER = (0, 1, -3, 3, 4, -2, 2, -1)
+ORDER = (0, 1, 4, -3, 3, -2, 2, -1)
 very_low = -1e30
 norm_eps = 1e-06
 
@@ -273,23 +272,18 @@
         beside(0)
     with jax.named_scope("attend0"):
         attend(0)
-    with jax.named_scope("w_across1"):
-        across(1)
     with jax.named_scope("w_three"):
         arrived(three)
     spread(three)
+    with jax.named_scope("w_across1"):
+        across(1)
+    with jax.named_scope("w_four"):
+        arrived(four)
+    spread(four)
     with jax.named_scope("w_beside1"):
         beside(1)
     with jax.named_scope("attend1"):
         attend(1)
-    with jax.named_scope("w_four"):
-        arrived(four)
-    spread(four)
-
-    @pl.when(c == 0)
-    def _():
-        with jax.named_scope("pass_down"):
-            pass_down()
 
     with jax.named_scope("w_across2"):
         across(2)
@@ -299,7 +293,6 @@
         beside(2)
     with jax.named_scope("attend2"):
         attend(2)
-
     with jax.named_scope("w_across4"):
         across(4)
     with jax.named_scope("w_beside3"):
@@ -313,19 +306,33 @@
     with jax.named_scope("attend4"):
         attend(4)
 
+    for load_w in loads[1:]:
+        load_w.wait()
+
+    @pl.when(c == 1)
+    def _():
+        loads[0].wait()
+
+
     with jax.named_scope("project"):
-        done = []
-        for head in range(HEADS):
-            summed = acc[head * TOK : (head + 1) * TOK, :]
-            done.append(summed / pltpu.roll(summed, HEAD_DIM, 1))
-        for pair in range(HEADS // 2):
-            moved = pltpu.roll(done[2 * pair], HEAD_DIM, 1)
-            att[:, pair * TOK : (pair + 1) * TOK] = jnp.where(lane < HEAD_DIM, moved, done[2 * pair + 1]).astype(BF16)
-        for step in (1, 3, 2):
-            other = (tp + step) % NT
-            remote(
-                att.at[pl.ds(pl.multiple_of(other * ROWS, ROWS), ROWS)], planes.at[tp], asend, arecv.at[tp], sp, other
-            ).start()
+        with jax.named_scope("p_heads"):
+            done = []
+            for head in range(HEADS):
+                summed = acc[head * TOK : (head + 1) * TOK, :]
+                done.append(summed / pltpu.roll(summed, HEAD_DIM, 1))
+            for pair in range(HEADS // 2):
+                moved = pltpu.roll(done[2 * pair], HEAD_DIM, 1)
+                att[:, pair * TOK : (pair + 1) * TOK] = jnp.where(lane < HEAD_DIM, moved, done[2 * pair + 1]).astype(BF16)
+            for step in (1, 3, 2):
+                other = (tp + step) % NT
+                remote(
+                    att.at[pl.ds(pl.multiple_of(other * ROWS, ROWS), ROWS)], planes.at[tp], asend, arecv.at[tp], sp, other
+                ).start()
+
+        @pl.when(c == 0)
+        def _():
+            pass_down()
+
         load.wait()
         in_copies["res"].wait()
         in_copies["gain"].wait()
@@ -340,15 +347,16 @@
             other = (tp + step) % NT
             remote(planes.at[other], planes.at[other], asend, arecv.at[other], sp, other).wait_recv()
             total = total + part_of(planes[other], other)
-        stream = (res_ref[...].astype(F32) + total).astype(BF16)
-        kept[...] = stream
-        stream = stream.astype(F32)
-        normed = stream * lax.rsqrt(jnp.mean(stream * stream, axis=1, keepdims=True) + norm_eps)
-        normed = (normed * gain_ref[...]).astype(BF16)
-        for piece in range(PIECES):
-            stacked[piece * ROWS : (piece + 1) * ROWS, :] = normed[:, piece * WIDE : (piece + 1) * WIDE]
-
-    for g in range(NZ):
+        with jax.named_scope("p_norm"):
+            stream = (res_ref[...].astype(F32) + total).astype(BF16)
+            kept[...] = stream
+            stream = stream.astype(F32)
+            normed = stream * lax.rsqrt(jnp.mean(stream * stream, axis=1, keepdims=True) + norm_eps)
+            normed = (normed * gain_ref[...]).astype(BF16)
+            for piece in range(PIECES):
+                stacked[piece * ROWS : (piece + 1) * ROWS, :] = normed[:, piece * WIDE : (piece + 1) * WIDE]
+
+    def dispatch(g):
         plane = (z - ORDER[g] + NZ) % NZ
         rows = pl.ds(pl.multiple_of(plane * TOK, TOK), TOK)
         picked = jnp.dot(chosen[rows, :], stacked[...], preferred_element_type=F32).astype(BF16)
@@ -489,22 +497,6 @@
             lax.fori_loop(0, PLANE, one_row, 0)
 
     chunks = NZ // 2
-    for g in range(AHEAD):
-        with jax.named_scope(f"share{g}"):
-            share(g)
-    for g in range(AHEAD, NZ):
-        with jax.named_scope(f"relay{g - AHEAD}"):
-            relay(g - AHEAD)
-        with jax.named_scope(f"share{g}"):
-            share(g)
-    for load_w in loads[1:]:
-        load_w.wait()
-
-    @pl.when(c == 1)
-    def _():
-        loads[0].wait()
-
-
     def first_return(chunk):
         @pl.when(c == 1)
         def _():
@@ -513,6 +505,13 @@
                     add_half(g)
 
     def last_return(chunk):
+        @pl.when(c == 1)
+        def _():
+            for g in (2 * chunk, 2 * chunk + 1):
+                with jax.named_scope(f"back{g}"):
+                    give_back(g)
+
+    def from_hidden(chunk):
         @pl.when(c == 0)
         def _():
             if chunk == 0:
@@ -521,13 +520,7 @@
             with jax.named_scope(f"finish{chunk}"):
                 finish(chunk)
 
-        @pl.when(c == 1)
-        def _():
-            for g in (2 * chunk, 2 * chunk + 1):
-                with jax.named_scope(f"back{g}"):
-                    give_back(g)
-
-    for chunk in range(chunks):
+    def expert(chunk):
         for g in (2 * chunk, 2 * chunk + 1):
             with jax.named_scope(f"gathered{g}"):
                 gathered(g)
@@ -535,28 +528,48 @@
             compute(chunk)
 
         @pl.when(c == 0)
-        def _(chunk=chunk):
+        def _():
             send_hidden(chunk)
 
         @pl.when(c == 1)
-        def _(chunk=chunk):
+        def _():
             with jax.named_scope(f"multiply{chunk}"):
                 multiply(chunk)
             first_halves(2 * chunk)
             first_halves(2 * chunk + 1)
 
-        if chunk < 2:
-            for g in (2 * chunk + AHEAD, 2 * chunk + AHEAD + 1):
-                with jax.named_scope(f"relay{g}"):
-                    relay(g)
-        if chunk > 0:
-            first_return(chunk - 1)
-        if chunk > 1:
-            last_return(chunk - 2)
-    last_return(chunks - 2)
-    first_return(chunks - 1)
-    last_return(chunks - 1)
-
+    D_, S, R, E, H, A, B = dispatch, share, relay, expert, from_hidden, first_return, last_return
+    for step, number in (
+        (D_, 0), (D_, 1), (D_, 2), (D_, 3), (D_, 4), (S, 0), (D_, 5), (D_, 6), (D_, 7), (S, 1), (R, 0), (S, 2), (S, 3),
+        (R, 1), (R, 2), (S, 4), (S, 5), (E, 0), (R, 3), (S, 6), (S, 7), (A, 0), (R, 4), (R, 5), (H, 0), (E, 1),
+        (R, 6), (R, 7), (E, 2), (H, 1), (A, 1), (B, 0), (E, 3), (H, 2), (A, 2), (B, 1), (H, 3), (A, 3), (B, 2), (B, 3),
+    ):
+        with jax.named_scope(f"{step.__name__}{number}"):
+            step(number)
+
+    some = sent.at[pl.ds(0, experts - 1)]
+    remote(some, some, dsend, drecv.at[0], sp, right).wait_send()
+    some = came.at[pl.ds(0, 3)]
+    remote(some, some, ysend, yl.at[0], sp, right).wait_send()
+
+    @pl.when(c == 0)
+    def _():
+        some = w_down.at[pl.ds(0, 3)]
+        remote(some, some, gsend, gl.at[0], sp, right).wait_send()
+        some = hid_in.at[pl.ds(0, 6)]
+        remote(some, some, hsend, hrecv.at[0], sp, right).wait_send()
+
+    @pl.when(c == 1)
+    def _():
+        some = pieces.at[pl.ds(0, 6)]
+        remote(some, some, rsend, ra.at[0], sp, right).wait_send()
+
+
+    count = 5 + 15 + 20
+    remote(kvg.at[pl.ds(0, count)], kvg.at[pl.ds(0, count)], send, recv.at[0], sp, (tp + 1) % NT).wait_send()
+    remote(planes.at[pl.ds(0, 3)], planes.at[pl.ds(0, 3)], asend, arecv.at[0], sp, (tp + 1) % NT).wait_send()
+
+    columns = turn[...].T[0:ROWS, :]
     total = jnp.zeros((2 * PIECES * ROWS, WIDE), F32)
     for g in range(NZ):
         plane = (z - ORDER[g] + NZ) % NZ
@@ -565,7 +578,6 @@
             remote(ref, ref, fsend, frecv.at[plane], sp, right).wait_recv()
         rows = final[pl.ds(pl.multiple_of(plane * PLANE, PLANE), PLANE)].reshape(TOK, WIDE)
         total = total + jnp.dot(pick[plane], rows, preferred_element_type=F32)
-    columns = turn[...].T[0:ROWS, :]
     weight0, weight1 = columns[:, 2:3], columns[:, 3:4]
     for piece in range(PIECES):
         lanes = slice(piece * WIDE, (piece + 1) * WIDE)
@@ -573,29 +585,8 @@
         two = total[(PIECES + piece) * ROWS : (PIECES + piece + 1) * ROWS]
         out_ref[:, lanes] = (kept[:, lanes].astype(F32) + (weight0 * one + weight1 * two)).astype(BF16)
 
-    some = sent.at[pl.ds(0, experts - 1)]
-    remote(some, some, dsend, drecv.at[0], sp, right).wait_send()
-    some = came.at[pl.ds(0, 3)]
-    remote(some, some, ysend, yl.at[0], sp, right).wait_send()
-
-    @pl.when(c == 0)
-    def _():
-        some = w_down.at[pl.ds(0, 3)]
-        remote(some, some, gsend, gl.at[0], sp, right).wait_send()
-        some = hid_in.at[pl.ds(0, 6)]
-        remote(some, some, hsend, hrecv.at[0], sp, right).wait_send()
-
-    @pl.when(c == 1)
-    def _():
-        some = pieces.at[pl.ds(0, 6)]
-        remote(some, some, rsend, ra.at[0], sp, right).wait_send()
-
     some = final.at[pl.ds(0, experts - 1)]
     remote(some, some, fsend, frecv.at[0], sp, right).wait_send()
-
-    count = 5 + 15 + 20
-    remote(kvg.at[pl.ds(0, count)], kvg.at[pl.ds(0, count)], send, recv.at[0], sp, (tp + 1) % NT).wait_send()
-    remote(planes.at[pl.ds(0, 3)], planes.at[pl.ds(0, 3)], asend, arecv.at[0], sp, (tp + 1) % NT).wait_send()
 
 
 def local(

time: 84.6 us -> 82.1 us (0.970)
  Pallas kernels: 83 us -> 80.4 us
    pallas_call x1, Pallas kernels: 83 us -> 80.4 us  [local(): pl.pallas_call(layer_kernel, out_shape=jax.ShapeDtypeStruct((ROWS, D), BF...]
where the time goes in v3:
time: 82.1 us; the launch traced here: 82 us
  Pallas kernels  80.4 us (98%)
  local copies, waits for them, and re-layouts  1.57 us (2%)
    pallas_call x1, Pallas kernels, local(): pl.pallas_call(layer_kernel, out_shape=jax.ShapeDtypeStruct((ROWS, D), BF...  80.4 us

profile of v3, /device:TPU:1, one launch (start us, length us, event | category | flops | bytes accessed | tf_op | source)
XLA Modules:
  0.0 82.0 jit_solution(6980653678972220261)
XLA Ops:
  0.0 80.4 %layer.1 = bf16[32,2048]{1,0:T(8,128)(2,1)} custom-call(bf16[128,256]{1,0:T(8,128)(2,1)} %q_hbm.1, bf16[64,128]{1,0:T(8,128)(2,1)} %bitcast.7, bf16[64,128]{1,0:T(8,128)(2,1)} %bitcast.8, f32[4,128]{1,0:T(4,128)} %bitcast.10, s32[1,128]{1,0:T(1,128)} %bitcast.13, bf16[32,2048]{1,0:T(8,128)(2,1)} %res_hbm.1, f32[1,2048]{1,0:T(1,128)} %bitcast.9, ...), custom_call_target="tpu_custom_call" | custom-call | tf_op jit(solution)/shard_map/layer/pallas_call | solution.py:599
  80.4 1.6 %copy.15 = bf16[32,2048]{1,0:T(8,128)(2,1)} copy(bf16[32,2048]{1,0:T(8,128)(2,1)} %layer.1) | data formatting | bytes 262144

commit v4 on v3

--- a/solution.py
+++ b/solution.py
@@ -22,6 +22,7 @@
 WIDE = 256
 PIECES = D // WIDE
 ORDER = (0, 1, 4, -3, 3, -2, 2, -1)
+PAIRS = ((0, 2), (3, 4), (5, 6), (1, 7))
 very_low = -1e30
 norm_eps = 1e-06
 
@@ -52,7 +53,7 @@
     q_ref, gates_ref, doc_ref, res_ref, gain_ref, ids_ref, weights_ref,
     kvg, aux, qs, bias, top, acc, soft, turned_v, att, planes, proj, kept, stacked,
     turn, chosen, choose, sent, came, pick, xrows, w_gate, w_up, w_down,
-    hidden, hid_out, hid_in, pieces, half_l, half_r, full_l, full_r, to_r, to_l, back, final,
+    hidden, hid_out, hid_in, pieces, half_l, half_r, full_l, full_r, to_r, to_l, back, final, taken,
     insem, recv, send, arecv, asend, psem,
     wsem, dsend, drecv, ysend, yl, yr, ya, yb, rsend, ra, rb, rl, rr, fsend, frecv,
     gsend, gl, gr, hsend, hrecv,
@@ -61,6 +62,16 @@
     right, left, far = (tp + 1) % NT, (tp + 3) % NT, (tp + 2) % NT
     experts = NZ * PLANE
     barrier = pltpu.get_barrier_semaphore()
+    for step in range(1, NT):
+        pl.semaphore_signal(barrier, inc=1, device_id=at(sp, (tp + step) % NT), device_id_type=MESH)
+
+    def greet(turn_of, carry):
+        for part in range(7):
+            other = (sp + 1 + turn_of * 7 + part) % experts
+            pl.semaphore_signal(barrier, inc=1, device_id=at(other, tp), device_id_type=MESH)
+        return carry
+
+    lax.fori_loop(0, (experts - 1) // 7, greet, 0)
     in_copies = {}
     for k, (name, hbm, vmem) in enumerate((
         ("k", k_hbm, kvg.at[sp, pl.ds(0, HEAD_DIM)]), ("v", v_hbm, kvg.at[sp, pl.ds(HEAD_DIM, HEAD_DIM)]),
@@ -70,13 +81,6 @@
         in_copies[name] = pltpu.make_async_copy(hbm, vmem, insem.at[k])
         in_copies[name].start()
 
-    def greet(step, carry):
-        pl.semaphore_signal(barrier, inc=1, device_id=at((sp + step) % experts, tp), device_id_type=MESH)
-        return carry
-
-    lax.fori_loop(1, experts, greet, 0)
-    for step in range(1, NT):
-        pl.semaphore_signal(barrier, inc=1, device_id=at(sp, (tp + step) % NT), device_id_type=MESH)
     load = pltpu.make_async_copy(proj_hbm, proj, psem)
     load.start()
     loads = [
@@ -363,7 +367,7 @@
         sent[pl.ds(pl.multiple_of(plane * PLANE, PLANE), PLANE)] = picked.reshape(PLANE, 16, WIDE)
 
         def one_row(k, carry, plane=plane):
-            target = plane * PLANE + k
+            target = plane * PLANE + (x * NC + c + k) % PLANE
             remote(sent.at[target], came.at[tp, sp], dsend, drecv.at[z], target, tp).start()
             return carry
 
@@ -407,7 +411,7 @@
 
     def compute(chunk):
         for k in range(2):
-            plane = plane_at(2 * chunk + k)
+            plane = plane_at(PAIRS[chunk][k])
             for source in range(NT):
                 rows = came[source, pl.ds(pl.multiple_of(plane * PLANE, PLANE), PLANE)].reshape(TOK, WIDE)
                 ordered = jnp.dot(choose[0], rows, preferred_element_type=F32).astype(BF16)
@@ -424,11 +428,11 @@
         for k in range(2):
             for source in range(NT):
                 q = (k * NT + source) * 16
-                pieces[2 * chunk + k, source] = part[q : q + 16, :]
+                pieces[PAIRS[chunk][k], source] = part[q : q + 16, :]
 
     def send_hidden(chunk):
         for k in range(2):
-            g = 2 * chunk + k
+            g = PAIRS[chunk][k]
             for source in range(NT):
                 q = (k * NT + source) * 16
                 hid_out[g, source] = hidden[q : q + 16, :]
@@ -438,16 +442,16 @@
 
     def finish(chunk):
         for k in range(2):
-            g = 2 * chunk + k
+            g = PAIRS[chunk][k]
             some = hid_in.at[g, pl.ds(0, NT - 1)]
             remote(some, some, hsend, hrecv.at[g], sp, right).wait_recv()
         total = jnp.zeros((32, D), F32)
         for source in range(NT):
-            rows = hid_in[2 * chunk : 2 * chunk + 2, source].reshape(32, WIDE)
+            rows = jnp.concatenate([hid_in[g, source] for g in PAIRS[chunk]], axis=0)
             total = total + jnp.dot(rows, w_down[source], preferred_element_type=F32)
         total = total.astype(BF16)
         for k in range(2):
-            hand_back(2 * chunk + k, total[16 * k : 16 * k + 16, :])
+            hand_back(PAIRS[chunk][k], total[16 * k : 16 * k + 16, :])
 
     half = D // 2
 
@@ -481,6 +485,7 @@
         back[pl.ds(pl.multiple_of(g * PLANE, PLANE), PLANE)] = mixed.reshape(PLANE, 16, WIDE)
 
         def one_row(k, carry):
+            k = (x * NC + c + k) % PLANE
             target = plane * PLANE + k
             remote(back.at[g * PLANE + k], final.at[sp], fsend, frecv.at[z], target, tp).start()
             return carry
@@ -500,14 +505,14 @@
     def first_return(chunk):
         @pl.when(c == 1)
         def _():
-            for g in (2 * chunk, 2 * chunk + 1):
+            for g in PAIRS[chunk]:
                 with jax.named_scope(f"add_half{g}"):
                     add_half(g)
 
     def last_return(chunk):
         @pl.when(c == 1)
         def _():
-            for g in (2 * chunk, 2 * chunk + 1):
+            for g in PAIRS[chunk]:
                 with jax.named_scope(f"back{g}"):
                     give_back(g)
 
@@ -521,7 +526,7 @@
                 finish(chunk)
 
     def expert(chunk):
-        for g in (2 * chunk, 2 * chunk + 1):
+        for g in PAIRS[chunk]:
             with jax.named_scope(f"gathered{g}"):
                 gathered(g)
         with jax.named_scope(f"compute{chunk}"):
@@ -535,14 +540,14 @@
         def _():
             with jax.named_scope(f"multiply{chunk}"):
                 multiply(chunk)
-            first_halves(2 * chunk)
-            first_halves(2 * chunk + 1)
+            for g in PAIRS[chunk]:
+                first_halves(g)
 
     D_, S, R, E, H, A, B = dispatch, share, relay, expert, from_hidden, first_return, last_return
     for step, number in (
         (D_, 0), (D_, 1), (D_, 2), (D_, 3), (D_, 4), (S, 0), (D_, 5), (D_, 6), (D_, 7), (S, 1), (R, 0), (S, 2), (S, 3),
-        (R, 1), (R, 2), (S, 4), (S, 5), (E, 0), (R, 3), (S, 6), (S, 7), (A, 0), (R, 4), (R, 5), (H, 0), (E, 1),
-        (R, 6), (R, 7), (E, 2), (H, 1), (A, 1), (B, 0), (E, 3), (H, 2), (A, 2), (B, 1), (H, 3), (A, 3), (B, 2), (B, 3),
+        (R, 1), (R, 2), (S, 4), (S, 5), (S, 6), (S, 7), (R, 3), (E, 0), (R, 4), (R, 5), (R, 6), (R, 7), (A, 0), (E, 1),
+        (E, 2), (H, 0), (A, 1), (B, 0), (E, 3), (H, 1), (A, 2), (B, 1), (H, 2), (A, 3), (B, 2), (H, 3), (B, 3),
     ):
         with jax.named_scope(f"{step.__name__}{number}"):
             step(number)
@@ -570,19 +575,19 @@
     remote(planes.at[pl.ds(0, 3)], planes.at[pl.ds(0, 3)], asend, arecv.at[0], sp, (tp + 1) % NT).wait_send()
 
     columns = turn[...].T[0:ROWS, :]
-    total = jnp.zeros((2 * PIECES * ROWS, WIDE), F32)
-    for g in range(NZ):
+    for first, g in enumerate(g for pair in PAIRS for g in pair):
         plane = (z - ORDER[g] + NZ) % NZ
         ref = final.at[pl.ds(pl.multiple_of(plane * PLANE, PLANE), PLANE)]
         with jax.named_scope(f"take{g}"):
             remote(ref, ref, fsend, frecv.at[plane], sp, right).wait_recv()
         rows = final[pl.ds(pl.multiple_of(plane * PLANE, PLANE), PLANE)].reshape(TOK, WIDE)
-        total = total + jnp.dot(pick[plane], rows, preferred_element_type=F32)
+        part = jnp.dot(pick[plane], rows, preferred_element_type=F32)
+        taken[...] = part if first == 0 else taken[...] + part
     weight0, weight1 = columns[:, 2:3], columns[:, 3:4]
     for piece in range(PIECES):
         lanes = slice(piece * WIDE, (piece + 1) * WIDE)
-        one = total[piece * ROWS : (piece + 1) * ROWS]
-        two = total[(PIECES + piece) * ROWS : (PIECES + piece + 1) * ROWS]
+        one = taken[piece * ROWS : (piece + 1) * ROWS, :]
+        two = taken[(PIECES + piece) * ROWS : (PIECES + piece + 1) * ROWS, :]
         out_ref[:, lanes] = (kept[:, lanes].astype(F32) + (weight0 * one + weight1 * two)).astype(BF16)
 
     some = final.at[pl.ds(0, experts - 1)]
@@ -598,7 +603,7 @@
     wide_heads = HEADS * HEAD_DIM
     return pl.pallas_call(
         layer_kernel,
-        out_shape=jax.ShapeDtypeStruct((ROWS, D), BF16),
+        out_shape=pltpu.VMEM((ROWS, D), BF16),
         in_specs=[anywhere] * 13,
         out_specs=pl.BlockSpec(memory_space=pltpu.VMEM),
         scratch_shapes=[
@@ -644,6 +649,7 @@
             pltpu.VMEM((NZ, 16, D), BF16),
             pltpu.VMEM((experts, 16, WIDE), BF16),
             pltpu.VMEM((experts, 16, WIDE), BF16),
+            pltpu.VMEM((2 * PIECES * ROWS, WIDE), F32),
             dma((9,)), dma((experts,)), dma, dma((NT,)), dma, dma,
             dma((3,)), dma, dma((NZ,)), dma, dma((NZ,)), dma((NZ,)), dma((NZ,)), dma((NZ,)),
             dma, dma((NZ,)), dma((NZ,)), dma((NZ,)), dma((NZ,)), dma, dma((NZ,)),

time: 82.1 us -> 80.5 us (0.981)
  local copies, waits for them, and re-layouts: 1.57 us -> 0.66 us
    unnamed x1, local copies, waits for them, and re-layouts: 1.57 us -> 0.66 us
where the time goes in v4:
time: 80.5 us; the launch traced here: 80.3 us
  Pallas kernels  79.7 us (99%)
    pallas_call x1, Pallas kernels, local(): pl.pallas_call(layer_kernel, out_shape=pltpu.VMEM((ROWS, D), BF16), in_sp...  79.7 us

profile of v4, /device:TPU:1, one launch (start us, length us, event | category | flops | bytes accessed | tf_op | source)
XLA Modules:
  0.0 80.3 jit_solution(14438015897618253663)
XLA Ops:
  0.0 79.7 %layer.1 = bf16[32,2048]{1,0:T(8,128)(2,1)S(1)} custom-call(bf16[128,256]{1,0:T(8,128)(2,1)} %q_hbm.1, bf16[64,128]{1,0:T(8,128)(2,1)} %bitcast.7, bf16[64,128]{1,0:T(8,128)(2,1)} %bitcast.8, f32[4,128]{1,0:T(4,128)} %bitcast.10, s32[1,128]{1,0:T(1,128)} %bitcast.13, bf16[32,2048]{1,0:T(8,128)(2,1)} %res_hbm.1, f32[1,2048]{1,0:T(1,128)} %bitcast.9, ...), custom_call_target="tpu_custom_call" | custom-call | tf_op jit(solution)/shard_map/layer/pallas_call | solution.py:604
  79.7 0.7 copy.15

commit v5 on v4

--- a/solution.py
+++ b/solution.py
@@ -327,7 +327,7 @@
             for pair in range(HEADS // 2):
                 moved = pltpu.roll(done[2 * pair], HEAD_DIM, 1)
                 att[:, pair * TOK : (pair + 1) * TOK] = jnp.where(lane < HEAD_DIM, moved, done[2 * pair + 1]).astype(BF16)
-            for step in (1, 3, 2):
+            for step in (2, 1, 3):
                 other = (tp + step) % NT
                 remote(
                     att.at[pl.ds(pl.multiple_of(other * ROWS, ROWS), ROWS)], planes.at[tp], asend, arecv.at[tp], sp, other
@@ -547,7 +547,7 @@
     for step, number in (
         (D_, 0), (D_, 1), (D_, 2), (D_, 3), (D_, 4), (S, 0), (D_, 5), (D_, 6), (D_, 7), (S, 1), (R, 0), (S, 2), (S, 3),
         (R, 1), (R, 2), (S, 4), (S, 5), (S, 6), (S, 7), (R, 3), (E, 0), (R, 4), (R, 5), (R, 6), (R, 7), (A, 0), (E, 1),
-        (E, 2), (H, 0), (A, 1), (B, 0), (E, 3), (H, 1), (A, 2), (B, 1), (H, 2), (A, 3), (B, 2), (H, 3), (B, 3),
+        (H, 0), (E, 2), (B, 0), (A, 1), (E, 3), (H, 1), (A, 2), (B, 1), (H, 2), (A, 3), (B, 2), (H, 3), (B, 3),
     ):
         with jax.named_scope(f"{step.__name__}{number}"):
             step(number)

time: 80.5 us -> 80.4 us (level)
  no operation moved by 1% of the time
where the time goes in v5:
time: 80.4 us; the launch traced here: 80.2 us
  Pallas kernels  79.6 us (99%)
    pallas_call x1, Pallas kernels, local(): pl.pallas_call(layer_kernel, out_shape=pltpu.VMEM((ROWS, D), BF16), in_sp...  79.6 us

profile of v5, /device:TPU:1, one launch (start us, length us, event | category | flops | bytes accessed | tf_op | source)
XLA Modules:
  0.0 80.2 jit_solution(4245414656886669857)
XLA Ops:
  0.0 79.6 %layer.1 = bf16[32,2048]{1,0:T(8,128)(2,1)S(1)} custom-call(bf16[128,256]{1,0:T(8,128)(2,1)} %q_hbm.1, bf16[64,128]{1,0:T(8,128)(2,1)} %bitcast.7, bf16[64,128]{1,0:T(8,128)(2,1)} %bitcast.8, f32[4,128]{1,0:T(4,128)} %bitcast.10, s32[1,128]{1,0:T(1,128)} %bitcast.13, bf16[32,2048]{1,0:T(8,128)(2,1)} %res_hbm.1, f32[1,2048]{1,0:T(1,128)} %bitcast.9, ...), custom_call_target="tpu_custom_call" | custom-call | tf_op jit(solution)/shard_map/layer/pallas_call | solution.py:604
  79.6 0.7 copy.15
